TPU v7x, 32 devices: a whole 2x2x4 slice. The times are simulated.
32 devices in a mesh: sp: 8 (over z, x), tp: 4 (over y, core).
Axes of the slice: x: 2, y: 2, z: 4, core: 2. Of those that a mesh axis runs over, the one named last changes fastest.
Arguments:
- residual: bfloat16 [2048, 2048], P('sp', 'tp'), may hold values from -8 to 8
- query_latent: bfloat16 [2048, 512], P('sp'), may hold values from -6 to 6
- shared_latent: bfloat16 [2048, 256], P('sp'), may hold values from -6 to 6
- rotary_key: bfloat16 [2048, 32], P('sp'), may hold values from -300 to 300
- query_gain: float32 [512], replicated, may hold values from 0.1 to 1.9
- latent_gain: float32 [256], replicated, may hold values from 0.1 to 1.9
- query_narrow: bfloat16 [512, 384], P(None, 'tp'), may hold values from -0.5 to 0.5
- key_narrow: bfloat16 [256, 256], P(None, 'tp'), may hold values from -0.375 to 0.375
- value_narrow: bfloat16 [256, 256], P(None, 'tp'), may hold values from -0.375 to 0.375
- query_wide: bfloat16 [512, 640], P(None, 'tp'), may hold values from -0.5 to 0.5
- key_wide: bfloat16 [256, 512], P(None, 'tp'), may hold values from -0.375 to 0.375
- value_wide: bfloat16 [256, 512], P(None, 'tp'), may hold values from -0.375 to 0.375
- output_narrow: bfloat16 [256, 2048], P('tp'), may hold values from -1.75 to 1.75
- output_wide: bfloat16 [512, 2048], P('tp'), may hold values from -1.75 to 1.75
- first_gain: float32 [2048], P('tp'), may hold values from 0.1 to 1.9
- first_bias: float32 [2048], P('tp'), may hold values from -1.5 to 1.5
- gate_weight: bfloat16 [2048, 5632], P('sp', 'tp'), may hold values from -0.125 to 0.125
- up_weight: bfloat16 [2048, 5632], P('sp', 'tp'), may hold values from -0.125 to 0.125
- down_weight: bfloat16 [5632, 2048], P('tp', 'sp'), may hold values from -0.078125 to 0.078125
- second_gain: float32 [2048], P('tp'), may hold values from 0.1 to 1.9
- second_bias: float32 [2048], P('tp'), may hold values from -1.5 to 1.5
Outputs:
- layer_out: bfloat16 [2048, 2048], P('sp', 'tp')
All inputs are finite; a program needn't handle non-finite values.
Results may differ from a plain program's by a relative error of at most 0.017.
The roundings to bfloat16 on the way count: a program that leaves them out, or rounds other values in their place, can miss the bound.
Values may be sent and summed in bfloat16 or wider, within the bound.
No kernel may reach another device: no remote copies, remote signals or barrier semaphores. Data moves between devices by JAX's collectives and lax.ppermute only.
A program may use at most 192 MiB of HBM per device.

v0:
```python
import jax
import jax.numpy as jnp
from jax import lax
from jax.sharding import PartitionSpec as P

ROPE = 32
NOPE_A = 64
V_A = 64
NOPE_B = 128
V_B = 128
GRID_W = 64


EPS_ROOT = 1e-06
EPS_LAYER = 1e-05
THETA = 10000.0
DEEP_ALPHA = 2.0**0.25


def rotate(half_part, angle):
    lower, upper = jnp.split(half_part, 2, axis=-1)
    cosine = jnp.cos(angle)
    sine = jnp.sin(angle)
    return jnp.concatenate([lower * cosine - upper * sine, upper * cosine + lower * sine], axis=-1)


def turn_axial(values_in, positions):
    quarter = values_in.shape[-1] // 4
    freqs = THETA ** (-(2.0 * jnp.arange(quarter, dtype=jnp.float32)) / (2 * quarter))
    row_angle = (positions // GRID_W).astype(jnp.float32)[:, None, None] * freqs
    col_angle = (positions % GRID_W).astype(jnp.float32)[:, None, None] * freqs
    first_half, second_half = jnp.split(values_in, 2, axis=-1)
    return jnp.concatenate([rotate(first_half, row_angle), rotate(second_half, col_angle)], axis=-1)


def root_scale(latent, gain):
    floated = latent.astype(jnp.float32)
    return (
        floated * lax.rsqrt(jnp.mean(floated * floated, axis=-1, keepdims=True) + EPS_ROOT) * gain
    )


def make_query(normed, weight, plain_dim, positions):
    product = jnp.dot(normed, weight, preferred_element_type=jnp.float32)
    head_count = weight.shape[1] // (plain_dim + ROPE)
    product = product.reshape(product.shape[0], head_count, plain_dim + ROPE)
    turned = turn_axial(product[:, :, plain_dim:], positions)
    return jnp.concatenate([product[:, :, :plain_dim], turned], axis=-1).astype(jnp.bfloat16)


def fresh_state(row_count, head_count, value_dim):
    largest = jnp.full((head_count, row_count), -jnp.inf, jnp.float32)
    totals = jnp.zeros((head_count, row_count), jnp.float32)
    weighted = jnp.zeros((row_count, head_count, value_dim), jnp.float32)
    return (largest, totals, weighted)


def update(state_now, queries, key_rows, value_rows, rotary_rows, plain_dim):
    largest, totals, weighted = state_now
    score_scale = queries.shape[2] ** (-0.5)
    scores = jnp.einsum(
        "qhd,khd->hqk", queries[:, :, :plain_dim], key_rows, preferred_element_type=jnp.float32
    )
    scores = scores + jnp.einsum(
        "qhd,kd->hqk", queries[:, :, plain_dim:], rotary_rows, preferred_element_type=jnp.float32
    )
    scores = scores * score_scale
    new_largest = jnp.max(scores, axis=-1)
    factor = jnp.exp(largest - new_largest)
    raised = jnp.exp(scores - new_largest[:, :, None])
    totals = totals * factor + jnp.sum(raised, axis=-1)
    added = jnp.einsum(
        "hqk,khd->qhd", raised.astype(jnp.bfloat16), value_rows, preferred_element_type=jnp.float32
    )
    weighted = weighted * factor.T[:, :, None] + added
    return (new_largest, totals, weighted)


def finish(state_now):
    largest, totals, weighted = state_now
    output = (weighted / totals.T[:, :, None]).astype(jnp.bfloat16)
    return output.reshape(output.shape[0], output.shape[1] * output.shape[2])


def finish_norm(summed, sums, squares, gain, bias, width_total):
    center = sums / width_total
    spread = squares / width_total - center * center
    normed = (summed - center[:, None]) * lax.rsqrt(spread + EPS_LAYER)[:, None]
    return (normed * gain + bias).astype(jnp.bfloat16)


def body(
    residual,
    query_latent,
    shared_latent,
    rotary_key,
    query_gain,
    latent_gain,
    query_narrow,
    key_narrow,
    value_narrow,
    query_wide,
    key_wide,
    value_wide,
    output_narrow,
    output_wide,
    first_gain,
    first_bias,
    gate_weight,
    up_weight,
    down_weight,
    second_gain,
    second_bias,
):
    row_count = residual.shape[0]
    offset = lax.axis_index("sp") * row_count
    positions = offset + jnp.arange(row_count, dtype=jnp.int32)
    query_normed = root_scale(query_latent, query_gain).astype(jnp.bfloat16)
    narrow_queries = make_query(query_normed, query_narrow, NOPE_A, positions)
    wide_queries = make_query(query_normed, query_wide, NOPE_B, positions)
    narrow_heads = narrow_queries.shape[1]
    wide_heads = wide_queries.shape[1]
    start_state = (
        fresh_state(row_count, narrow_heads, V_A),
        fresh_state(row_count, wide_heads, V_B),
    )
    shard_rows = (
        lax.all_gather(shared_latent, "sp", axis=0, tiled=True),
        lax.all_gather(rotary_key, "sp", axis=0, tiled=True),
    )
    latent_rows = shard_rows[0]
    normed = root_scale(latent_rows, latent_gain).astype(jnp.bfloat16)
    count = latent_rows.shape[0]
    narrow_keys = jnp.dot(normed, key_narrow, preferred_element_type=jnp.float32).astype(
        jnp.bfloat16
    )
    narrow_vals = jnp.dot(normed, value_narrow, preferred_element_type=jnp.float32).astype(
        jnp.bfloat16
    )
    wide_keys = jnp.dot(normed, key_wide, preferred_element_type=jnp.float32).astype(jnp.bfloat16)
    wide_vals = jnp.dot(normed, value_wide, preferred_element_type=jnp.float32).astype(jnp.bfloat16)
    key_positions = jnp.arange(count, dtype=jnp.int32)
    rotated = turn_axial(shard_rows[1].astype(jnp.float32)[:, None, :], key_positions)[
        :, 0, :
    ].astype(jnp.bfloat16)
    count = rotated.shape[0]
    narrow_state = update(
        start_state[0],
        narrow_queries,
        narrow_keys.reshape(count, narrow_heads, NOPE_A),
        narrow_vals.reshape(count, narrow_heads, V_A),
        rotated,
        NOPE_A,
    )
    wide_state = update(
        start_state[1],
        wide_queries,
        wide_keys.reshape(count, wide_heads, NOPE_B),
        wide_vals.reshape(count, wide_heads, V_B),
        rotated,
        NOPE_B,
    )
    narrow_out = finish(narrow_state)
    wide_out = finish(wide_state)
    terms = jnp.dot(narrow_out, output_narrow, preferred_element_type=jnp.float32)
    terms = terms + jnp.dot(wide_out, output_wide, preferred_element_type=jnp.float32)
    mixed = lax.psum_scatter(
        terms.astype(jnp.bfloat16), "tp", scatter_dimension=1, tiled=True
    ).astype(jnp.float32)
    width_total = mixed.shape[1] * lax.axis_size("tp")
    summed = DEEP_ALPHA * residual.astype(jnp.float32) + mixed
    sums, squares = lax.psum((jnp.sum(summed, axis=1), jnp.sum(summed * summed, axis=1)), "tp")
    normed_first = finish_norm(summed, sums, squares, first_gain, first_bias, width_total)
    full_rows = lax.all_gather(normed_first, "tp", axis=1, tiled=True)
    shard_rows = (
        lax.all_gather(gate_weight, "sp", axis=0, tiled=True),
        lax.all_gather(up_weight, "sp", axis=0, tiled=True),
    )
    gate_part = jnp.dot(full_rows, shard_rows[0], preferred_element_type=jnp.float32)
    lifted_part = jnp.dot(full_rows, shard_rows[1], preferred_element_type=jnp.float32)
    hidden = (jax.nn.silu(gate_part) * lifted_part).astype(jnp.bfloat16)
    feed_terms = jnp.dot(
        hidden,
        lax.all_gather(down_weight, "sp", axis=1, tiled=True),
        preferred_element_type=jnp.float32,
    )
    feed = lax.psum_scatter(
        feed_terms.astype(jnp.bfloat16), "tp", scatter_dimension=1, tiled=True
    ).astype(jnp.float32)
    summed_two = DEEP_ALPHA * normed_first.astype(jnp.float32) + feed
    sums_two, squares_two = lax.psum(
        (jnp.sum(summed_two, axis=1), jnp.sum(summed_two * summed_two, axis=1)), "tp"
    )
    return finish_norm(summed_two, sums_two, squares_two, second_gain, second_bias, width_total)


def solution(mesh):
    return jax.shard_map(
        body,
        mesh=mesh,
        in_specs=(
            P("sp", "tp"),
            P("sp", None),
            P("sp", None),
            P("sp", None),
            P(),
            P(),
            P(None, "tp"),
            P(None, "tp"),
            P(None, "tp"),
            P(None, "tp"),
            P(None, "tp"),
            P(None, "tp"),
            P("tp", None),
            P("tp", None),
            P("tp"),
            P("tp"),
            P("sp", "tp"),
            P("sp", "tp"),
            P("tp", "sp"),
            P("tp"),
            P("tp"),
        ),
        out_specs=P("sp", "tp"),
        check_vma=False,
    )
```

profile of v0, /device:TPU:0, one launch (start us, length us, event | category | flops | bytes accessed | tf_op | source)
XLA Modules:
  0.0 453.0 jit_solution(9527016040940097273)
XLA Ops:
  6.5 0.7 all-gather.6.cloned.1.call-update
  7.3 0.0 reduce-scatter.3.cloned.1.call-start
  7.4 32.8 %all_gather.19 = bf16[2048,32]{0,1:T(8,128)(2,1)S(1)} all-gather(bf16[256,32]{0,1:T(8,128)(2,1)} %param.24), channel_id=1, replica_groups=mesh['sp'=8,'tp'=4] {'sp'}, dimensions={0}, use_global_device_ids=true | all-gather | bytes 147456 | tf_op jit(solution)/shard_map/all_gather | solution.py:129
  40.2 1.1 fusion.31
  41.3 1.3 convolution_bitcast_fusion.5
  42.6 1.3 convolution_bitcast_fusion.4
  43.9 0.2 fusion.97
  44.1 0.6 fusion.59
  44.7 7.9 %all-gather.6.cloned.1.call-done = bf16[2048,256]{1,0:T(8,128)(2,1)} async-done(((bf16[256,256]{1,0:T(8,128)(2,1)}), bf16[2048,256]{1,0:T(8,128)(2,1)}) %all-gather.6.cloned.1.call-update) | async-done | bytes 1048592 | tf_op jit(solution)/shard_map/all_gather | solution.py:128
  52.5 1.6 fusion.6
  54.1 2.1 convolution_bitcast_fusion.3
  56.3 0.6 fusion.132
  56.9 1.3 copy-done.2
  58.2 0.4 fusion.9
  58.6 0.2 copy-done.1
  58.8 2.2 convolution_bitcast_fusion.1
  61.1 2.1 fusion.131
  63.2 1.3 copy-done.3
  64.6 0.4 fusion.11
  65.0 2.6 fusion.20
  67.6 1.8 fusion.133
  69.4 2.6 fusion.24
  72.1 3.1 fusion.4
  75.2 0.0 reduce-scatter.3.cloned.1.call-update
  75.2 0.0 all-gather.8.cloned.1.call-start
  75.2 23.7 %reduce-scatter.3.cloned.1.call-done = bf16[256,512]{1,0:T(8,128)(2,1)} async-done(((bf16[256,2048]{1,0:T(8,128)(2,1)}), bf16[256,512]{1,0:T(8,128)(2,1)}) %reduce-scatter.3.cloned.1.call-update) | async-done | bytes 262160 | tf_op jit(solution)/shard_map/reduce_scatter | solution.py:167
  99.0 1.2 fusion.34
  100.1 5.8 %all-reduce.1 = (f32[256]{0:T(256)S(1)}, f32[256]{0:T(256)S(1)}) all-reduce(f32[256]{0:T(256)S(1)} %get-tuple-element.8, f32[256]{0:T(256)S(1)} %get-tuple-element.7), channel_id=1, replica_groups=mesh['sp'=8,'tp'=4] {'tp'}, use_global_device_ids=true, to_apply=%region_10.11 | all-reduce | flops 512 | bytes 4096 | tf_op jit(solution)/shard_map/psum | solution.py:172
  105.9 1.8 add_convert_fusion.1
  107.7 0.0 all-gather.8.cloned.1.call-update
  107.7 0.0 all-gather.10.cloned.1.call-start
  107.8 0.5 all-gather.10.cloned.1.call-update
  108.3 0.0 all-gather.12.cloned.1.call-start
  108.4 0.5 all-gather.12.cloned.1.call-update
  108.9 0.0 all-gather.14.cloned.1.call-start
  109.0 0.5 all-gather.14.cloned.1.call-update
  109.5 0.2 reduce-scatter.5.cloned.1.call-start
  109.7 15.5 %all-gather.8.cloned.1.call-done = bf16[256,2048]{1,0:T(8,128)(2,1)} async-done(((bf16[256,512]{1,0:T(8,128)(2,1)}), bf16[256,2048]{1,0:T(8,128)(2,1)}) %all-gather.8.cloned.1.call-update) | async-done | bytes 1048592 | tf_op jit(solution)/shard_map/all_gather | solution.py:174
  125.2 94.4 %all-gather.10.cloned.1.call-done = bf16[2048,1408]{1,0:T(8,128)(2,1)} async-done(((bf16[256,1408]{1,0:T(8,128)(2,1)}), bf16[2048,1408]{1,0:T(8,128)(2,1)}) %all-gather.10.cloned.1.call-update) | async-done | bytes 5767184 | tf_op jit(solution)/shard_map/all_gather | solution.py:176
  219.6 4.8 %fusion.134 = f32[256,1408]{1,0:T(8,128)S(1)} fusion(bf16[256,2048]{1,0:T(8,128)(2,1)} %all-gather.8.cloned.1.call-done, bf16[2048,1408]{1,0:T(8,128)(2,1)} %all-gather.10.cloned.1.call-done), kind=kOutput, calls=%fused_computation.179 | convolution fusion | flops 1476395008 | bytes 8257536 | tf_op jit(solution)/shard_map/dot_general | solution.py:179
  224.4 87.8 %all-gather.12.cloned.1.call-done = bf16[2048,1408]{1,0:T(8,128)(2,1)} async-done(((bf16[256,1408]{1,0:T(8,128)(2,1)}), bf16[2048,1408]{1,0:T(8,128)(2,1)}) %all-gather.12.cloned.1.call-update) | async-done | bytes 5767184 | tf_op jit(solution)/shard_map/all_gather | solution.py:177
  312.2 93.2 %all-gather.14.cloned.1.call-done = bf16[1408,2048]{1,0:T(8,128)(2,1)} async-done(((bf16[1408,256]{1,0:T(8,128)(2,1)}), bf16[1408,2048]{1,0:T(8,128)(2,1)}) %all-gather.14.cloned.1.call-update) | async-done | bytes 5767184 | tf_op jit(solution)/shard_map/all_gather | solution.py:184
  405.4 8.8 %convolution_convert_fusion = bf16[256,2048]{1,0:T(8,128)(2,1)} fusion(bf16[1408,2048]{1,0:T(8,128)(2,1)} %all-gather.14.cloned.1.call-done, bf16[256,2048]{1,0:T(8,128)(2,1)S(1)} %copy-done.14, bf16[2048,1408]{1,0:T(8,128)(2,1)} %all-gather.12.cloned.1.call-done, f32[256,1408]{1,0:T(8,128)S(1)} %fusion.134), kind=kOutput, calls=%fused_computation.14 | convolution fusion | flops 2955476992 | bytes 15073280 | tf_op jit(solution)/shard_map/dot_general | solution.py:182
  414.2 0.0 reduce-scatter.5.cloned.1.call-update
  414.2 23.1 %reduce-scatter.5.cloned.1.call-done = bf16[256,512]{1,0:T(8,128)(2,1)} async-done(((bf16[256,2048]{1,0:T(8,128)(2,1)}), bf16[256,512]{1,0:T(8,128)(2,1)}) %reduce-scatter.5.cloned.1.call-update) | async-done | bytes 262160 | tf_op jit(solution)/shard_map/reduce_scatter | solution.py:187
  437.4 1.2 fusion.35
  438.5 5.8 %all-reduce = (f32[256]{0:T(256)S(1)}, f32[256]{0:T(256)S(1)}) all-reduce(f32[256]{0:T(256)S(1)} %get-tuple-element.6, f32[256]{0:T(256)S(1)} %get-tuple-element.5), channel_id=1, replica_groups=mesh['sp'=8,'tp'=4] {'tp'}, use_global_device_ids=true, to_apply=%region_15.16 | all-reduce | flops 512 | bytes 4096 | tf_op jit(solution)/shard_map/psum | solution.py:191
  444.3 1.8 add_convert_fusion
  (42 shorter events, 0.2 us)
Async XLA Ops:
  6.5 61.1 %copy-start = (bf16[128,2048]{1,0:T(8,128)(2,1)S(1)}, bf16[128,2048]{1,0:T(8,128)(2,1)}, u32[]{:S(2)}) copy-start(bf16[128,2048]{1,0:T(8,128)(2,1)} %param.34) | copy-start | bytes 1572868
  6.5 47.6 %copy-start.9 = (f32[256]{0:T(256)S(1)}, f32[256]{0:T(256)}, u32[]{:S(2)}) copy-start(f32[256]{0:T(256)} %param.26) | copy-start | bytes 3076
  6.5 47.6 %copy-start.8 = (bf16[256,64]{0,1:T(8,128)(2,1)S(1)}, bf16[256,64]{0,1:T(8,128)(2,1)}, u32[]{:S(2)}) copy-start(bf16[256,64]{0,1:T(8,128)(2,1)} %param.28) | copy-start | bytes 98308
  6.5 46.0 %all-gather.6.cloned.1.call-start = ((), (), s32[]{:S(2)}) async-start(), calls=%async_computation.2 | async-start | bytes 1179648 | tf_op jit(solution)/shard_map/all_gather | solution.py:128
  7.3 91.7 %reduce-scatter.3.cloned.1.call-start = ((), (), s32[]{:S(2)}) async-start(), calls=%async_computation.3 | async-start | bytes 1310720 | tf_op jit(solution)/shard_map/reduce_scatter | solution.py:167
  56.8 1.3 copy-start.2
  56.9 2.0 copy-start.1
  56.9 2.0 copy-start.7
  63.2 1.3 copy-start.3
  63.2 1.8 copy-start.15
  67.6 1.8 copy-start.16
  69.4 2.6 copy-start.6
  72.1 26.9 %copy-start.5 = (bf16[256,512]{1,0:T(8,128)(2,1)S(1)}, bf16[256,512]{1,0:T(8,128)(2,1)}, u32[]{:S(2)}) copy-start(bf16[256,512]{1,0:T(8,128)(2,1)} %param.21) | copy-start | bytes 786436
  72.1 33.8 %copy-start.10 = (f32[512]{0:T(512)S(1)}, f32[512]{0:T(512)}, u32[]{:S(2)}) copy-start(f32[512]{0:T(512)} %param.36) | copy-start | bytes 6148
  72.1 33.8 %copy-start.11 = (f32[512]{0:T(512)S(1)}, f32[512]{0:T(512)}, u32[]{:S(2)}) copy-start(f32[512]{0:T(512)} %param.35) | copy-start | bytes 6148
  75.2 50.0 %all-gather.8.cloned.1.call-start = ((), (), s32[]{:S(2)}) async-start(), calls=%async_computation.4 | async-start | bytes 1310720 | tf_op jit(solution)/shard_map/all_gather | solution.py:174
  107.7 111.8 %all-gather.10.cloned.1.call-start = ((), (), s32[]{:S(2)}) async-start(), calls=%async_computation.5 | async-start | bytes 6488064 | tf_op jit(solution)/shard_map/all_gather | solution.py:176
  108.3 203.8 %all-gather.12.cloned.1.call-start = ((), (), s32[]{:S(2)}) async-start(), calls=%async_computation.6 | async-start | bytes 6488064 | tf_op jit(solution)/shard_map/all_gather | solution.py:177
  108.9 296.5 %all-gather.14.cloned.1.call-start = ((), (), s32[]{:S(2)}) async-start(), calls=%async_computation.7 | async-start | bytes 6488064 | tf_op jit(solution)/shard_map/all_gather | solution.py:184
  109.5 327.9 %reduce-scatter.5.cloned.1.call-start = ((), (), s32[]{:S(2)}) async-start(), calls=%async_computation.8 | async-start | bytes 1310720 | tf_op jit(solution)/shard_map/reduce_scatter | solution.py:187
  125.2 280.2 %copy-start.14 = (bf16[256,2048]{1,0:T(8,128)(2,1)S(1)}, bf16[256,2048]{1,0:T(8,128)(2,1)}, u32[]{:S(2)}) copy-start(bf16[256,2048]{1,0:T(8,128)(2,1)} %all-gather.8.cloned.1.call-done) | copy-start | bytes 3145732
  224.4 213.0 %copy-start.4 = (bf16[256,512]{1,0:T(8,128)(2,1)S(1)}, bf16[256,512]{1,0:T(8,128)(2,1)}, u32[]{:S(2)}) copy-start(bf16[256,512]{1,0:T(8,128)(2,1)} %add_convert_fusion.1) | copy-start | bytes 786436
  224.4 219.9 %copy-start.12 = (f32[512]{0:T(512)S(1)}, f32[512]{0:T(512)}, u32[]{:S(2)}) copy-start(f32[512]{0:T(512)} %param.41) | copy-start | bytes 6148
  224.4 219.9 %copy-start.13 = (f32[512]{0:T(512)S(1)}, f32[512]{0:T(512)}, u32[]{:S(2)}) copy-start(f32[512]{0:T(512)} %param.40) | copy-start | bytes 6148
Sparse Core Ops, SparseCore 0:
  9.5 43.0 all-gather.5
  75.3 23.6 reduce-scatter.2
  107.9 17.3 all-gather.7
  127.3 92.2 all-gather.9
  221.6 90.4 all-gather.11
  314.0 91.2 all-gather.13
  414.4 22.9 reduce-scatter.4
where the time goes:
time: 454 us; the launch traced here: 453 us
  waiting for transfers between devices  348 us (77%)
  blocking collectives  44.4 us (10%)
  matrix products  33.3 us (7%)
  between operations  13.7 us (3%)
  other arithmetic  10.3 us (2%)
    all_gather x1, waiting for transfers between devices, body(): lax.all_gather(gate_weight, 'sp', axis=0, tiled=True)  94.4 us
    all_gather x1, waiting for transfers between devices, body(): lax.all_gather(down_weight, 'sp', axis=1, tiled=True)  93.2 us
    all_gather x1, waiting for transfers between devices, body(): lax.all_gather(up_weight, 'sp', axis=0, tiled=True)  87.8 us
    all_gather x1, blocking collectives, body(): lax.all_gather(rotary_key, 'sp', axis=0, tiled=True)  32.8 us
    reduce_scatter x1, waiting for transfers between devices, body(): lax.psum_scatter(terms.astype(jnp.bfloat16), 'tp', scatter_dimension=1, t...  23.7 us
    reduce_scatter x1, waiting for transfers between devices, body(): lax.psum_scatter(feed_terms.astype(jnp.bfloat16), 'tp', scatter_dimension...  23.1 us
    all_gather x1, waiting for transfers between devices, body(): full_rows = lax.all_gather(normed_first, 'tp', axis=1, tiled=True)  15.5 us
  transfers between devices with their start and end apart: 7, of which 7 were waited for; matrix products, arithmetic and copies ran while one was open for 2% of the time, Pallas kernels for 0%

commit v1 on v0

v1 whole, which is shorter than its diff:
```python
import jax
import jax.numpy as jnp
from jax import lax
from jax.sharding import PartitionSpec as P

ROPE = 32
NOPE_A = 64
NOPE_B = 128
GRID_W = 64


EPS_ROOT = 1e-06
EPS_LAYER = 1e-05
THETA = 10000.0
DEEP_ALPHA = 2.0**0.25


def rotate(half_part, angle):
    lower, upper = jnp.split(half_part, 2, axis=-1)
    cosine = jnp.cos(angle)
    sine = jnp.sin(angle)
    return jnp.concatenate([lower * cosine - upper * sine, upper * cosine + lower * sine], axis=-1)


def turn_axial(values_in, positions):
    quarter = values_in.shape[-1] // 4
    freqs = THETA ** (-(2.0 * jnp.arange(quarter, dtype=jnp.float32)) / (2 * quarter))
    row_angle = (positions // GRID_W).astype(jnp.float32)[:, None, None] * freqs
    col_angle = (positions % GRID_W).astype(jnp.float32)[:, None, None] * freqs
    first_half, second_half = jnp.split(values_in, 2, axis=-1)
    return jnp.concatenate([rotate(first_half, row_angle), rotate(second_half, col_angle)], axis=-1)


def root_scale(latent, gain):
    floated = latent.astype(jnp.float32)
    return (
        floated * lax.rsqrt(jnp.mean(floated * floated, axis=-1, keepdims=True) + EPS_ROOT) * gain
    )


def make_query(normed, weight, plain_dim, positions):
    product = jnp.dot(normed, weight, preferred_element_type=jnp.float32)
    head_count = weight.shape[1] // (plain_dim + ROPE)
    product = product.reshape(product.shape[0], head_count, plain_dim + ROPE)
    turned = turn_axial(product[:, :, plain_dim:], positions)
    return jnp.concatenate([product[:, :, :plain_dim], turned], axis=-1).astype(jnp.bfloat16)


def attend(queries, keys, values, rotated, plain_dim):
    score_scale = queries.shape[2] ** (-0.5)
    scores = jnp.einsum(
        "qhd,khd->hqk", queries[:, :, :plain_dim], keys, preferred_element_type=jnp.float32
    )
    scores = scores + jnp.einsum(
        "qhd,kd->hqk", queries[:, :, plain_dim:], rotated, preferred_element_type=jnp.float32
    )
    scores = scores * score_scale
    largest = jnp.max(scores, axis=-1, keepdims=True)
    raised = jnp.exp(scores - largest)
    totals = jnp.sum(raised, axis=-1)
    weighted = jnp.einsum(
        "hqk,khd->qhd", raised.astype(jnp.bfloat16), values, preferred_element_type=jnp.float32
    )
    output = (weighted / totals.T[:, :, None]).astype(jnp.bfloat16)
    return output.reshape(output.shape[0], output.shape[1] * output.shape[2])


def swap(value, axis, bit):
    count = lax.axis_size(axis)
    return lax.ppermute(value, axis, [(i, i ^ bit) for i in range(count)])


def tp_bits():
    bits = []
    bit = 1
    while bit < lax.axis_size("tp"):
        bits.append(bit)
        bit *= 2
    return bits


def gather_blocks(own):
    blocks = {0: own}
    for bit in reversed(tp_bits()):
        for q in list(blocks):
            blocks[q ^ bit] = swap(blocks[q], "tp", bit)
    return blocks


def fold_tp(blocks, bits):
    for bit in bits:
        sent = [q for q in sorted(blocks) if q & bit]
        packed = jnp.concatenate([blocks[q].astype(jnp.bfloat16) for q in sent], axis=1)
        got = swap(packed, "tp", bit)
        width = got.shape[1] // len(sent)
        blocks = {
            q ^ bit: blocks[q ^ bit]
            + got[:, n * width : (n + 1) * width].astype(jnp.float32)
            for n, q in enumerate(sent)
        }
    return blocks


def layer_stats(summed):
    stats = jnp.stack([jnp.sum(summed, axis=1), jnp.sum(summed * summed, axis=1)])
    total = lax.psum(stats, "tp")
    return total[0], total[1]


def finish_norm(summed, sums, squares, gain, bias, width_total):
    center = sums / width_total
    spread = squares / width_total - center * center
    normed = (summed - center[:, None]) * lax.rsqrt(spread + EPS_LAYER)[:, None]
    return (normed * gain + bias).astype(jnp.bfloat16)


def body(
    residual,
    query_latent,
    shared_latent,
    rotary_key,
    query_gain,
    latent_gain,
    query_narrow,
    key_narrow,
    value_narrow,
    query_wide,
    key_wide,
    value_wide,
    output_narrow,
    output_wide,
    first_gain,
    first_bias,
    gate_weight,
    up_weight,
    down_weight,
    second_gain,
    second_bias,
):
    row_count = residual.shape[0]
    sp_count = lax.axis_size("sp")
    tp_count = lax.axis_size("tp")
    sp_index = lax.axis_index("sp").astype(jnp.uint32)
    tp_index = lax.axis_index("tp").astype(jnp.uint32)
    low = (sp_index >> 1) & 1

    part = row_count // tp_count
    part_at = tp_index * part
    own_latent = lax.dynamic_slice_in_dim(shared_latent, part_at, part, 0)
    own_rotary = lax.dynamic_slice_in_dim(rotary_key, part_at, part, 0)
    part_positions = (sp_index * row_count + part_at).astype(jnp.int32) + jnp.arange(
        part, dtype=jnp.int32
    )
    own_normed = root_scale(own_latent, latent_gain).astype(jnp.bfloat16)
    own_rotated = turn_axial(own_rotary.astype(jnp.float32)[:, None, :], part_positions)[
        :, 0, :
    ].astype(jnp.bfloat16)
    own_rows = jnp.concatenate([own_normed, own_rotated], axis=1)
    all_rows = lax.all_gather(own_rows, ("sp", "tp"), axis=0, tiled=True)

    half = gate_weight.shape[1] // 2

    def pack(which):
        gate_half = lax.dynamic_slice_in_dim(gate_weight, which * half, half, 1)
        up_half = lax.dynamic_slice_in_dim(up_weight, which * half, half, 1)
        return jnp.concatenate([gate_half, up_half], axis=1)

    pairs = (pack(low), pack(1 - low))
    downs = tuple(
        lax.dynamic_slice_in_dim(down_weight, which * half, half, 0) for which in (low, 1 - low)
    )
    feature_width = residual.shape[1]
    block_width = gate_weight.shape[0]
    ratio = jnp.uint32(feature_width // block_width)

    def spread(sources):
        found = {}
        for step in range(sp_count // 2):
            found[step * 2] = sources[0] if step == 0 else swap(sources[step % 2], "sp", step * 2)
            found[step * 2 + 1] = swap(found[step * 2], "sp", 1)
        return found

    gate_up_blocks = spread(pairs)
    down_blocks = spread(downs)

    def place(blocks, axis, shape):
        whole = jnp.zeros(shape, jnp.bfloat16)
        for step, block in blocks.items():
            index = sp_index ^ step
            at = (lax.div(index, ratio) ^ tp_index) * feature_width
            at = at + lax.rem(index, ratio) * block_width
            whole = lax.dynamic_update_slice_in_dim(whole, block, at, axis)
        return whole

    positions = (sp_index * row_count).astype(jnp.int32) + jnp.arange(row_count, dtype=jnp.int32)
    query_normed = root_scale(query_latent, query_gain).astype(jnp.bfloat16)
    narrow_queries = make_query(query_normed, query_narrow, NOPE_A, positions)
    wide_queries = make_query(query_normed, query_wide, NOPE_B, positions)
    narrow_heads = narrow_queries.shape[1]
    wide_heads = wide_queries.shape[1]
    kv_width = shared_latent.shape[1]
    normed = all_rows[:, :kv_width]
    rotated = all_rows[:, kv_width:]
    count = all_rows.shape[0]

    def up(weight, heads):
        made = jnp.dot(normed, weight, preferred_element_type=jnp.float32).astype(jnp.bfloat16)
        return made.reshape(count, heads, weight.shape[1] // heads)

    narrow_out = attend(
        narrow_queries,
        up(key_narrow, narrow_heads),
        up(value_narrow, narrow_heads),
        rotated,
        NOPE_A,
    )
    wide_out = attend(
        wide_queries, up(key_wide, wide_heads), up(value_wide, wide_heads), rotated, NOPE_B
    )
    attended = jnp.concatenate([narrow_out, wide_out], axis=1)
    output_weight = jnp.concatenate([output_narrow, output_wide], axis=0)
    terms = {}
    for q in range(tp_count):
        piece = lax.dynamic_slice_in_dim(
            output_weight, (tp_index ^ q) * feature_width, feature_width, 1
        )
        terms[q] = jnp.dot(attended, piece, preferred_element_type=jnp.float32)
    mixed = fold_tp(terms, tp_bits())[0]
    width_total = feature_width * tp_count
    summed = DEEP_ALPHA * residual.astype(jnp.float32) + mixed
    sums, squares = layer_stats(summed)
    normed_first = finish_norm(summed, sums, squares, first_gain, first_bias, width_total)

    mate_first = swap(normed_first, "sp", 2)
    own_blocks = gather_blocks(normed_first)
    mate_blocks = gather_blocks(mate_first)
    rows_in = jnp.concatenate(
        [
            jnp.concatenate([own_blocks[q] for q in range(tp_count)], axis=1),
            jnp.concatenate([mate_blocks[q] for q in range(tp_count)], axis=1),
        ],
        axis=0,
    )
    gate_up = place(gate_up_blocks, 0, (width_total, 2 * half))
    both = jnp.dot(rows_in, gate_up, preferred_element_type=jnp.float32)
    hidden = (jax.nn.silu(both[:, :half]) * both[:, half:]).astype(jnp.bfloat16)
    down = place(down_blocks, 1, (half, width_total))
    feed_terms = {
        q: jnp.dot(
            hidden,
            down[:, q * feature_width : (q + 1) * feature_width],
            preferred_element_type=jnp.float32,
        )
        for q in range(tp_count)
    }
    bits = tp_bits()
    feed_terms = fold_tp(feed_terms, bits[:-1])
    kept = sorted(feed_terms)
    packed = jnp.concatenate([feed_terms[q][row_count:].astype(jnp.bfloat16) for q in kept], axis=1)
    got = swap(packed, "sp", 2)
    feed_terms = {
        q: feed_terms[q][:row_count]
        + got[:, n * feature_width : (n + 1) * feature_width].astype(jnp.float32)
        for n, q in enumerate(kept)
    }
    feed = fold_tp(feed_terms, bits[-1:])[0]
    summed_two = DEEP_ALPHA * normed_first.astype(jnp.float32) + feed
    sums_two, squares_two = layer_stats(summed_two)
    return finish_norm(summed_two, sums_two, squares_two, second_gain, second_bias, width_total)


def solution(mesh):
    return jax.shard_map(
        body,
        mesh=mesh,
        in_specs=(
            P("sp", "tp"),
            P("sp", None),
            P("sp", None),
            P("sp", None),
            P(),
            P(),
            P(None, "tp"),
            P(None, "tp"),
            P(None, "tp"),
            P(None, "tp"),
            P(None, "tp"),
            P(None, "tp"),
            P("tp", None),
            P("tp", None),
            P("tp"),
            P("tp"),
            P("sp", "tp"),
            P("sp", "tp"),
            P("tp", "sp"),
            P("tp"),
            P("tp"),
        ),
        out_specs=P("sp", "tp"),
        check_vma=False,
    )
```

time: 454 us -> 265 us (0.58)
  waiting for transfers between devices: 348 us -> 123 us
  starting transfers between devices: 0.42 us -> 43.6 us
  blocking collectives: 44.4 us -> 11.9 us
  local copies, waits for them, and re-layouts: 2.91 us -> 28.1 us
    all_gather x5 -> x1, waiting for transfers between devices: 299 us -> 31.9 us  [body(): all_rows = lax.all_gather(own_rows, ('sp', 'tp'), axis=0, tiled=True)]
    ppermute x0 -> x26, waiting for transfers between devices: none -> 91.4 us  [swap(): return lax.ppermute(value, axis, [(i, i ^ bit) for i in range(count)])]
    reduce_scatter x2 -> x0, waiting for transfers between devices: 46.8 us -> none  [the longest x1 23.7 us: body(): lax.psum_scatter(terms.astype(jnp.bfloat16), 'tp', scatter_dimension=1, t...]
    ppermute x0 -> x26, starting transfers between devices: none -> 43.6 us  [swap(): return lax.ppermute(value, axis, [(i, i ^ bit) for i in range(count)])]
    all_gather x1 -> x0, blocking collectives: 32.8 us -> none  [body(): lax.all_gather(rotary_key, 'sp', axis=0, tiled=True)]
    dynamic_update_slice x0 -> x15, local copies, waits for them, and re-layouts: none -> 20 us  [place(): whole = lax.dynamic_update_slice_in_dim(whole, block, at, axis)]
    dot_general x10 -> x15, matrix products: 30.7 us -> 27.1 us  [the longest x2 7.04 us: attend(): jnp.einsum('qhd,khd->hqk', queries[:, :, :plain_dim], keys, preferred_ele...]
  transfers between devices with their start and end apart: 7 -> 27, of which waited for: 7 -> 13; matrix products, arithmetic and copies ran while one was open for 2% -> 21% of each run, Pallas kernels for 0% -> 0%
where the time goes in v1:
time: 265 us; the launch traced here: 264 us
  waiting for transfers between devices  123 us (46%)
  starting transfers between devices  43.6 us (16%)
  matrix products  29.6 us (11%)
  local copies, waits for them, and re-layouts  28.1 us (11%)
  between operations  13.9 us (5%)
  other arithmetic  13.1 us (5%)
  blocking collectives  11.9 us (4%)
    ppermute x26, waiting for transfers between devices, swap(): return lax.ppermute(value, axis, [(i, i ^ bit) for i in range(count)])  91.4 us
    ppermute x26, starting transfers between devices, swap(): return lax.ppermute(value, axis, [(i, i ^ bit) for i in range(count)])  43.6 us
    all_gather x1, waiting for transfers between devices, body(): all_rows = lax.all_gather(own_rows, ('sp', 'tp'), axis=0, tiled=True)  31.9 us
    dynamic_update_slice x15, local copies, waits for them, and re-layouts, place(): whole = lax.dynamic_update_slice_in_dim(whole, block, at, axis)  20 us
    psum x2, blocking collectives, layer_stats(): total = lax.psum(stats, 'tp')  11.9 us
    dot_general x2, matrix products, attend(): jnp.einsum('qhd,khd->hqk', queries[:, :, :plain_dim], keys, preferred_ele...  7.04 us
    dot_general x1, matrix products, body(): both = jnp.dot(rows_in, gate_up, preferred_element_type=jnp.float32)  6.04 us
    dot_general x2, matrix products, attend(): jnp.einsum('qhd,kd->hqk', queries[:, :, plain_dim:], rotated, preferred_e...  5.75 us
  transfers between devices with their start and end apart: 27, of which 13 were waited for; matrix products, arithmetic and copies ran while one was open for 21% of the time, Pallas kernels for 0%

profile of v1, /device:TPU:0, one launch (start us, length us, event | category | flops | bytes accessed | tf_op | source)
XLA Modules:
  0.0 263.6 jit_solution(13408120660436848153)
XLA Ops:
  10.1 2.1 constant_dynamic-slice_fusion.2
  12.6 1.1 constant_dynamic-update-slice_fusion.15
  13.8 3.0 %collective-permute-start.9 = (bf16[256,1408]{1,0:T(8,128)(2,1)}, bf16[256,1408]{1,0:T(8,128)(2,1)}, u32[]{:S(2)}, u32[]{:S(2)}) collective-permute-start(bf16[256,1408]{1,0:T(8,128)(2,1)} %get-tuple-element.14), channel_id=1, source_target_pairs={{0,4},{4,0},{8,12},{12,8},{16,20},{20,16},{24,28},{28,24},{1,5},{5... | collective-permute-start | bytes 2162696 | tf_op jit(solution)/shard_map/ppermute | solution.py:70
  16.7 2.6 collective-permute-start.12
  20.4 1.6 collective-permute-start.10
  24.3 1.1 fusion.53
  25.4 1.3 convolution_bitcast_fusion.5
  26.7 1.3 convolution_bitcast_fusion.4
  28.0 1.7 constant_dynamic-update-slice_fusion.17
  29.7 1.4 fusion.107
  31.1 1.9 constant_dynamic-update-slice_fusion.16
  33.1 8.2 %collective-permute-done.16 = bf16[704,256]{1,0:T(8,128)(2,1)} collective-permute-done((bf16[704,256]{1,0:T(8,128)(2,1)}, bf16[704,256]{1,0:T(8,128)(2,1)}, u32[]{:S(2)}, u32[]{:S(2)}) %collective-permute-start.16) | collective-permute-done | bytes 360480 | tf_op jit(solution)/shard_map/ppermute | solution.py:70
  41.3 3.9 %collective-permute-start.14 = (bf16[256,1408]{1,0:T(8,128)(2,1)}, bf16[256,1408]{1,0:T(8,128)(2,1)}, u32[]{:S(2)}, u32[]{:S(2)}) collective-permute-start(bf16[256,1408]{1,0:T(8,128)(2,1)} %pad_maximum_fusion.2), channel_id=1, source_target_pairs={{0,24},{4,28},{8,16},{12,20},{16,8},{20,12},{24,0},{28,4},{1,25},{... | collective-permute-start | bytes 2162696 | tf_op jit(solution)/shard_map/ppermute | solution.py:70
  46.1 27.2 %collective-permute-done.17 = bf16[704,256]{1,0:T(8,128)(2,1)S(1)} collective-permute-done((bf16[704,256]{1,0:T(8,128)(2,1)}, bf16[704,256]{1,0:T(8,128)(2,1)S(1)}, u32[]{:S(2)}, u32[]{:S(2)}) %collective-permute-start.17) | collective-permute-done | bytes 360480 | tf_op jit(solution)/shard_map/ppermute | solution.py:70
  73.3 4.5 %collective-permute-start.19 = (bf16[704,256]{1,0:T(8,128)(2,1)}, bf16[704,256]{1,0:T(8,128)(2,1)}, u32[]{:S(2)}, u32[]{:S(2)}) collective-permute-start(bf16[704,256]{1,0:T(8,128)(2,1)} %get-tuple-element.11), channel_id=1, source_target_pairs={{0,16},{4,20},{8,24},{12,28},{16,0},{20,4},{24,8},{28,12},{1,17},{... | collective-permute-start | bytes 1081352 | tf_op jit(solution)/shard_map/ppermute | solution.py:70
  77.9 31.9 %all-gather.2.cloned.1.call-done = bf16[2048,288]{1,0:T(8,128)(2,1)} async-done(((bf16[64,288]{1,0:T(8,128)(2,1)}), bf16[2048,288]{1,0:T(8,128)(2,1)}) %all-gather.2.cloned.1.call-update) | async-done | bytes 1179664 | tf_op jit(solution)/shard_map/all_gather | solution.py:159
  109.8 2.9 %convolution_bitcast_fusion.2 = f32[1,256,2048]{2,1,0:T(8,128)} fusion(bf16[2048,288]{1,0:T(8,128)(2,1)} %all-gather.2.cloned.1.call-done, bf16[256,1,8]{0,2,1:T(8,128)(2,1)} %get-tuple-element.30, bf16[256,1,8]{0,2,1:T(8,128)(2,1)} %get-tuple-element.31, bf16[256,1,8]{0,2,1:T(8,128)(2,1)} %get-tuple-element.27, bf16[256,1,8]{0,2,1:T(8,128)(2,1)} %get-tuple-element.26), kind=kOutput, calls=%fused_computation.2 | convolution fusion | flops 33619968 | bytes 2637824 | tf_op jit(solution)/shard_map/qhd,kd->hqk/dot_general | solution.py:54
  112.7 2.9 %fusion.156 = (f32[256]{0:T(256)S(1)}, f32[1,256,2048]{2,1,0:T(8,128)S(1)}) fusion(f32[1,256,2048]{2,1,0:T(8,128)} %convolution_bitcast_fusion.2, bf16[256,64]{0,1:T(8,128)(2,1)S(1)} %copy-done.12, bf16[2048,288]{1,0:T(8,128)(2,1)} %all-gather.2.cloned.1.call-done, f32[256,1,96]{0,2,1:T(8,128)S(1)} %convolution_bitcast_fusion.5), kind=kOutput, calls=%fused_computation.243 | convolution fusion | flops 135921408 | bytes 5309440 | tf_op jit(solution)/shard_map/qhd,khd->hqk/dot_general | solution.py:51
  116.0 2.9 %convolution_bitcast_fusion = f32[1,256,2048]{2,1,0:T(8,128)} fusion(bf16[2048,288]{1,0:T(8,128)(2,1)} %all-gather.2.cloned.1.call-done, bf16[256,1,8]{0,2,1:T(8,128)(2,1)S(1)} %get-tuple-element.39, bf16[256,1,8]{0,2,1:T(8,128)(2,1)S(1)} %get-tuple-element.38, bf16[256,1,8]{0,2,1:T(8,128)(2,1)S(1)} %get-tuple-element.40, ...), kind=kOutput, calls=%fused_computation | convolution fusion | flops 33619968 | bytes 2637824 | tf_op jit(solution)/shard_map/qhd,kd->hqk/dot_general | solution.py:54
  118.9 4.2 %fusion.153 = (f32[256]{0:T(256)S(1)}, f32[1,256,2048]{2,1,0:T(8,128)}) fusion(f32[1,256,2048]{2,1,0:T(8,128)} %convolution_bitcast_fusion, bf16[256,128]{1,0:T(8,128)(2,1)S(1)} %copy-done.11, bf16[2048,288]{1,0:T(8,128)(2,1)} %all-gather.2.cloned.1.call-done, f32[256,1,160]{0,2,1:T(8,128)S(1)} %copy-done.10), kind=kOutput, calls=%fused_computation.242 | convolution fusion | flops 270270208 | bytes 5374976 | tf_op jit(solution)/shard_map/qhd,khd->hqk/dot_general | solution.py:51
  123.1 2.1 fusion.34
  125.2 2.1 fusion.22
  127.3 2.9 %fusion.31 = bf16[256,128]{0,1:T(8,128)(2,1)S(1)} fusion(bf16[256,128]{1,0:T(8,128)(2,1)S(1)} %copy-done.19, f32[1,256,2048]{2,1,0:T(8,128)} %get-tuple-element.47, f32[256]{0:T(256)S(1)} %get-tuple-element.46, bf16[2048,288]{1,0:T(8,128)(2,1)} %all-gather.2.cloned.1.call-done, f32[256]{0:T(256)S(1)} %fusion.22), kind=kOutput, calls=%fused_computation.50 | convolution fusion | flops 269811712 | bytes 3278848 | tf_op jit(solution)/shard_map/hqk,khd->qhd/dot_general | solution.py:61
  130.8 2.3 collective-permute-start.21
  134.0 2.0 constant_dynamic-update-slice_fusion.14
  136.0 2.1 constant_dynamic-update-slice_fusion.13
  138.1 5.5 %collective-permute-done.21 = bf16[704,256]{1,0:T(8,128)(2,1)} collective-permute-done((bf16[704,256]{1,0:T(8,128)(2,1)}, bf16[704,256]{1,0:T(8,128)(2,1)}, u32[]{:S(2)}, u32[]{:S(2)}) %collective-permute-start.21) | collective-permute-done | bytes 360480 | tf_op jit(solution)/shard_map/ppermute | solution.py:70
  144.5 1.1 collective-permute-start.22
  146.4 1.8 constant_dynamic-update-slice_fusion.3
  149.1 1.2 collective-permute-start.13
  151.4 3.7 %collective-permute-done.20 = bf16[704,256]{1,0:T(8,128)(2,1)S(1)} collective-permute-done((bf16[704,256]{1,0:T(8,128)(2,1)}, bf16[704,256]{1,0:T(8,128)(2,1)S(1)}, u32[]{:S(2)}, u32[]{:S(2)}) %collective-permute-start.20) | collective-permute-done | bytes 360480 | tf_op jit(solution)/shard_map/ppermute | solution.py:70
  156.8 1.8 constant_dynamic-update-slice_fusion.1
  158.8 2.7 %collective-permute-done.1 = bf16[256,512]{1,0:T(8,128)(2,1)S(1)} collective-permute-done((bf16[256,512]{1,0:T(8,128)(2,1)S(1)}, bf16[256,512]{1,0:T(8,128)(2,1)S(1)}, u32[]{:S(2)}, u32[]{:S(2)}) %collective-permute-start.1) | collective-permute-done | bytes 262176 | tf_op jit(solution)/shard_map/ppermute | solution.py:70
  161.7 6.1 %psum.14 = f32[2,256]{1,0:T(2,128)S(1)} all-reduce(f32[2,256]{1,0:T(2,128)S(1)} %pad_maximum_fusion.7), channel_id=1, replica_groups=mesh['sp'=8,'tp'=4] {'tp'}, use_global_device_ids=true, to_apply=%region_8.9 | all-reduce | flops 512 | bytes 4096 | tf_op jit(solution)/shard_map/psum | solution.py:106
  168.0 7.7 %collective-permute-start.5 = (bf16[256,512]{1,0:T(8,128)(2,1)S(1)}, bf16[256,512]{1,0:T(8,128)(2,1)S(1)}, u32[]{:S(2)}, u32[]{:S(2)}) collective-permute-start(bf16[256,512]{1,0:T(8,128)(2,1)S(1)} %add_convert_fusion.1), channel_id=1, source_target_pairs={{0,8},{4,12},{8,0},{12,4},{16,24},{20,28},{24,16},{28,20},{1,9},{5... | collective-permute-start | bytes 786440 | tf_op jit(solution)/shard_map/ppermute | solution.py:70
  175.8 1.8 constant_dynamic-update-slice_fusion
  180.1 1.7 collective-permute-done.5
  182.2 2.0 constant_dynamic-update-slice_fusion.11
  184.2 9.5 %collective-permute-done.13 = bf16[256,1408]{1,0:T(8,128)(2,1)S(1)} collective-permute-done((bf16[256,1408]{1,0:T(8,128)(2,1)}, bf16[256,1408]{1,0:T(8,128)(2,1)S(1)}, u32[]{:S(2)}, u32[]{:S(2)}) %collective-permute-start.13) | collective-permute-done | bytes 720928 | tf_op jit(solution)/shard_map/ppermute | solution.py:70
  195.6 2.0 constant_dynamic-update-slice_fusion.9
  197.7 9.8 %collective-permute-done.15 = bf16[256,1408]{1,0:T(8,128)(2,1)S(1)} collective-permute-done((bf16[256,1408]{1,0:T(8,128)(2,1)}, bf16[256,1408]{1,0:T(8,128)(2,1)S(1)}, u32[]{:S(2)}, u32[]{:S(2)}) %collective-permute-start.15) | collective-permute-done | bytes 720928 | tf_op jit(solution)/shard_map/ppermute | solution.py:70
  208.5 6.0 %fusion.4 = f32[512,1408]{1,0:T(8,128)S(1)} fusion(bf16[2048,1408]{1,0:T(8,128)(2,1)} %constant_dynamic-update-slice_fusion.8, bf16[256,512]{1,0:T(8,128)(2,1)S(1)} %collective-permute-done.8, bf16[256,512]{1,0:T(8,128)(2,1)S(1)} %collective-permute-done.7, bf16[256,512]{1,0:T(8,128)(2,1)S(1)} %collective-permute-done.6, ...), kind=kOutput, calls=%fused_computation.12 | convolution fusion | flops 2969567232 | bytes 10747904 | tf_op jit(solution)/shard_map/dot_general | solution.py:245
  215.0 1.3 copy-done.3
  217.7 2.6 %collective-permute-done.23 = bf16[512,1024]{1,0:T(8,128)(2,1)S(1)} collective-permute-done((bf16[512,1024]{1,0:T(8,128)(2,1)S(1)}, bf16[512,1024]{1,0:T(8,128)(2,1)S(1)}, u32[]{:S(2)}, u32[]{:S(2)}) %collective-permute-start.23) | collective-permute-done | bytes 1048608 | tf_op jit(solution)/shard_map/ppermute | solution.py:70
  221.7 7.9 %collective-permute-start.24 = (bf16[256,1024]{1,0:T(8,128)(2,1)S(1)}, bf16[256,1024]{1,0:T(8,128)(2,1)S(1)}, u32[]{:S(2)}, u32[]{:S(2)}) collective-permute-start(bf16[256,1024]{1,0:T(8,128)(2,1)S(1)} %pad_maximum_fusion.4), channel_id=1, source_target_pairs={{0,8},{4,12},{8,0},{12,4},{16,24},{20,28},{24,16},{28,20},{1,9},{5... | collective-permute-start | bytes 1572872 | tf_op jit(solution)/shard_map/ppermute | solution.py:70
  229.6 12.2 %collective-permute-done.24 = bf16[256,1024]{1,0:T(8,128)(2,1)S(1)} collective-permute-done((bf16[256,1024]{1,0:T(8,128)(2,1)S(1)}, bf16[256,1024]{1,0:T(8,128)(2,1)S(1)}, u32[]{:S(2)}, u32[]{:S(2)}) %collective-permute-start.24) | collective-permute-done | bytes 524320 | tf_op jit(solution)/shard_map/ppermute | solution.py:70
  241.9 7.8 %collective-permute-done.25 = bf16[256,512]{1,0:T(8,128)(2,1)S(1)} collective-permute-done((bf16[256,512]{1,0:T(8,128)(2,1)S(1)}, bf16[256,512]{1,0:T(8,128)(2,1)S(1)}, u32[]{:S(2)}, u32[]{:S(2)}) %collective-permute-start.25) | collective-permute-done | bytes 262176 | tf_op jit(solution)/shard_map/ppermute | solution.py:70
  250.1 5.8 %psum.15 = f32[2,256]{1,0:T(2,128)S(1)} all-reduce(f32[2,256]{1,0:T(2,128)S(1)} %pad_maximum_fusion.8), channel_id=1, replica_groups=mesh['sp'=8,'tp'=4] {'tp'}, use_global_device_ids=true, to_apply=%region_11.12 | all-reduce | flops 512 | bytes 4096 | tf_op jit(solution)/shard_map/psum | solution.py:106
  (123 shorter events, 26.7 us)
Async XLA Ops:
  6.5 20.1 %copy-start = (bf16[512,160]{0,1:T(8,128)(2,1)S(1)}, bf16[512,160]{0,1:T(8,128)(2,1)}, u32[]{:S(2)}) copy-start(bf16[512,160]{0,1:T(8,128)(2,1)} %param.30) | copy-start | bytes 491524
  6.5 103.3 %all-gather.2.cloned.1.call-start = ((), (), s32[]{:S(2)}) async-start(), calls=%async_computation | async-start | bytes 1622016 | tf_op jit(solution)/shard_map/all_gather | solution.py:159
  6.6 1.0 copy-start.18
  12.6 9.7 %copy-start.5 = (bf16[1408,256]{1,0:T(8,128)(2,1)S(1)}, bf16[1408,256]{1,0:T(8,128)(2,1)}, u32[]{:S(2)}) copy-start(bf16[1408,256]{1,0:T(8,128)(2,1)} %param.39) | copy-start | bytes 2162692
  13.8 9.5 %copy-start.1 = (bf16[2048,1408]{1,0:T(8,128)(2,1)}, bf16[2048,1408]{1,0:T(8,128)(2,1)S(1)}, u32[]{:S(2)}) copy-start(bf16[2048,1408]{1,0:T(8,128)(2,1)S(1)} %get-tuple-element.13) | copy-start | bytes 17301508
  13.8 119.4 %collective-permute-start.9 = (bf16[256,1408]{1,0:T(8,128)(2,1)}, bf16[256,1408]{1,0:T(8,128)(2,1)}, u32[]{:S(2)}, u32[]{:S(2)}) collective-permute-start(bf16[256,1408]{1,0:T(8,128)(2,1)} %get-tuple-element.14), channel_id=1, source_target_pairs={{0,4},{4,0},{8,12},{12,8},{16,20},{20,16},{24,28},{28,24},{1,5},{5... | collective-permute-start | bytes 2162696 | tf_op jit(solution)/shard_map/ppermute | solution.py:70
  16.7 131.5 %collective-permute-start.12 = (bf16[256,1408]{1,0:T(8,128)(2,1)}, bf16[256,1408]{1,0:T(8,128)(2,1)}, u32[]{:S(2)}, u32[]{:S(2)}) collective-permute-start(bf16[256,1408]{1,0:T(8,128)(2,1)} %get-tuple-element.14), channel_id=1, source_target_pairs={{0,16},{4,20},{8,24},{12,28},{16,0},{20,4},{24,8},{28,12},{1,17},{... | collective-permute-start | bytes 2162696 | tf_op jit(solution)/shard_map/ppermute | solution.py:70
  19.3 6.1 %copy-start.20 = (f32[512]{0:T(512)S(1)}, f32[512]{0:T(512)}, u32[]{:S(2)}) copy-start(f32[512]{0:T(512)} %param.25) | copy-start | bytes 6148
  20.4 113.6 %collective-permute-start.10 = (bf16[256,1408]{1,0:T(8,128)(2,1)}, bf16[256,1408]{1,0:T(8,128)(2,1)}, u32[]{:S(2)}, u32[]{:S(2)}) collective-permute-start(bf16[256,1408]{1,0:T(8,128)(2,1)} %pad_maximum_fusion.2), channel_id=1, source_target_pairs={{0,8},{4,12},{8,0},{12,4},{16,24},{20,28},{24,16},{28,20},{1,9},{5... | collective-permute-start | bytes 2162696 | tf_op jit(solution)/shard_map/ppermute | solution.py:70
  23.3 17.9 %collective-permute-start.16 = (bf16[704,256]{1,0:T(8,128)(2,1)}, bf16[704,256]{1,0:T(8,128)(2,1)}, u32[]{:S(2)}, u32[]{:S(2)}) collective-permute-start(bf16[704,256]{1,0:T(8,128)(2,1)} %get-tuple-element.11), channel_id=1, source_target_pairs={{0,4},{4,0},{8,12},{12,8},{16,20},{20,16},{24,28},{28,24},{1,5},{5... | collective-permute-start | bytes 1081352 | tf_op jit(solution)/shard_map/ppermute | solution.py:70
  23.8 49.5 %collective-permute-start.17 = (bf16[704,256]{1,0:T(8,128)(2,1)}, bf16[704,256]{1,0:T(8,128)(2,1)S(1)}, u32[]{:S(2)}, u32[]{:S(2)}) collective-permute-start(bf16[704,256]{1,0:T(8,128)(2,1)} %get-tuple-element.15), channel_id=1, source_target_pairs={{0,8},{4,12},{8,0},{12,4},{16,24},{20,28},{24,16},{28,20},{1,9},{5... | collective-permute-start | bytes 1081352 | tf_op jit(solution)/shard_map/ppermute | solution.py:70
  27.9 1.8 copy-start.9
  28.0 84.7 %copy-start.12 = (bf16[256,64]{0,1:T(8,128)(2,1)S(1)}, bf16[256,64]{0,1:T(8,128)(2,1)}, u32[]{:S(2)}) copy-start(bf16[256,64]{0,1:T(8,128)(2,1)} %param.28) | copy-start | bytes 98308
  41.3 107.8 %collective-permute-start.14 = (bf16[256,1408]{1,0:T(8,128)(2,1)}, bf16[256,1408]{1,0:T(8,128)(2,1)}, u32[]{:S(2)}, u32[]{:S(2)}) collective-permute-start(bf16[256,1408]{1,0:T(8,128)(2,1)} %pad_maximum_fusion.2), channel_id=1, source_target_pairs={{0,24},{4,28},{8,16},{12,20},{16,8},{20,12},{24,0},{28,4},{1,25},{... | collective-permute-start | bytes 2162696 | tf_op jit(solution)/shard_map/ppermute | solution.py:70
  73.3 42.3 %copy-start.6 = (bf16[704,256]{1,0:T(8,128)(2,1)}, bf16[704,256]{1,0:T(8,128)(2,1)S(1)}, u32[]{:S(2)}) copy-start(bf16[704,256]{1,0:T(8,128)(2,1)S(1)} %collective-permute-done.17) | copy-start | bytes 1081348
  73.3 57.5 %collective-permute-start.19 = (bf16[704,256]{1,0:T(8,128)(2,1)}, bf16[704,256]{1,0:T(8,128)(2,1)}, u32[]{:S(2)}, u32[]{:S(2)}) collective-permute-start(bf16[704,256]{1,0:T(8,128)(2,1)} %get-tuple-element.11), channel_id=1, source_target_pairs={{0,16},{4,20},{8,24},{12,28},{16,0},{20,4},{24,8},{28,12},{1,17},{... | collective-permute-start | bytes 1081352 | tf_op jit(solution)/shard_map/ppermute | solution.py:70
  77.9 31.9 %copy-start.2 = (bf16[704,2048]{1,0:T(8,128)(2,1)}, bf16[704,2048]{1,0:T(8,128)(2,1)S(1)}, u32[]{:S(2)}) copy-start(bf16[704,2048]{1,0:T(8,128)(2,1)S(1)} %constant_dynamic-update-slice_fusion.5) | copy-start | bytes 8650756
  115.6 3.3 %copy-start.10 = (f32[256,1,160]{0,2,1:T(8,128)S(1)}, f32[256,1,160]{0,2,1:T(8,128)}, u32[]{:S(2)}) copy-start(f32[256,1,160]{0,2,1:T(8,128)} %copy-done.9) | copy-start | bytes 491524
  115.6 3.3 %copy-start.11 = (bf16[256,128]{1,0:T(8,128)(2,1)S(1)}, bf16[256,128]{1,0:T(8,128)(2,1)}, u32[]{:S(2)}) copy-start(bf16[256,128]{1,0:T(8,128)(2,1)} %param.31) | copy-start | bytes 196612
  118.9 4.2 %copy-start.13 = (bf16[256,64]{0,1:T(8,128)(2,1)S(1)}, bf16[256,64]{0,1:T(8,128)(2,1)}, u32[]{:S(2)}) copy-start(bf16[256,64]{0,1:T(8,128)(2,1)} %param.29) | copy-start | bytes 98308
  123.1 4.2 %copy-start.19 = (bf16[256,128]{1,0:T(8,128)(2,1)S(1)}, bf16[256,128]{1,0:T(8,128)(2,1)}, u32[]{:S(2)}) copy-start(bf16[256,128]{1,0:T(8,128)(2,1)} %param.32) | copy-start | bytes 196612
  125.2 5.0 %copy-start.4 = (bf16[192,2048]{1,0:T(8,128)(2,1)S(1)}, bf16[192,2048]{1,0:T(8,128)(2,1)}, u32[]{:S(2)}) copy-start(bf16[192,2048]{1,0:T(8,128)(2,1)} %constant_dynamic-update-slice_fusion.16) | copy-start | bytes 2359300
  127.3 5.8 %copy-start.7 = (bf16[704,256]{1,0:T(8,128)(2,1)S(1)}, bf16[704,256]{1,0:T(8,128)(2,1)}, u32[]{:S(2)}) copy-start(bf16[704,256]{1,0:T(8,128)(2,1)} %copy-done.6) | copy-start | bytes 1081348
  130.8 12.8 %collective-permute-start.21 = (bf16[704,256]{1,0:T(8,128)(2,1)}, bf16[704,256]{1,0:T(8,128)(2,1)}, u32[]{:S(2)}, u32[]{:S(2)}) collective-permute-start(bf16[704,256]{1,0:T(8,128)(2,1)} %get-tuple-element.15), channel_id=1, source_target_pairs={{0,24},{4,28},{8,16},{12,20},{16,8},{20,12},{24,0},{28,4},{1,25},{... | collective-permute-start | bytes 1081352 | tf_op jit(solution)/shard_map/ppermute | solution.py:70
  133.1 11.4 %collective-permute-start.18 = (bf16[704,256]{1,0:T(8,128)(2,1)S(1)}, bf16[704,256]{1,0:T(8,128)(2,1)S(1)}, u32[]{:S(2)}, u32[]{:S(2)}) collective-permute-start(bf16[704,256]{1,0:T(8,128)(2,1)S(1)} %copy-done.7), channel_id=1, source_target_pairs={{0,4},{4,0},{8,12},{12,8},{16,20},{20,16},{24,28},{28,24},{1,5},{5... | collective-permute-start | bytes 1081352 | tf_op jit(solution)/shard_map/ppermute | solution.py:70
  134.0 16.3 %collective-permute-start = (bf16[256,1024]{1,0:T(8,128)(2,1)S(1)}, bf16[256,1024]{1,0:T(8,128)(2,1)S(1)}, u32[]{:S(2)}, u32[]{:S(2)}) collective-permute-start(bf16[256,1024]{1,0:T(8,128)(2,1)S(1)} %pad_maximum_fusion.3), channel_id=1, source_target_pairs={{0,1},{1,0},{2,3},{3,2},{4,5},{5,4},{6,7},{7,6},{8,9},{9,8},{10,11... | collective-permute-start | bytes 1572872 | tf_op jit(solution)/shard_map/ppermute | solution.py:70
  136.0 25.4 %copy-start.8 = (bf16[256,512]{1,0:T(8,128)(2,1)S(1)}, bf16[256,512]{1,0:T(8,128)(2,1)}, u32[]{:S(2)}) copy-start(bf16[256,512]{1,0:T(8,128)(2,1)} %param.21) | copy-start | bytes 786436
  143.6 11.5 %collective-permute-start.20 = (bf16[704,256]{1,0:T(8,128)(2,1)}, bf16[704,256]{1,0:T(8,128)(2,1)S(1)}, u32[]{:S(2)}, u32[]{:S(2)}) collective-permute-start(bf16[704,256]{1,0:T(8,128)(2,1)} %collective-permute-done.19), channel_id=1, source_target_pairs={{0,4},{4,0},{8,12},{12,8},{16,20},{20,16},{24,28},{28,24},{1,5},{5... | collective-permute-start | bytes 1081352 | tf_op jit(solution)/shard_map/ppermute | solution.py:70
  144.5 31.3 %collective-permute-start.22 = (bf16[704,256]{1,0:T(8,128)(2,1)}, bf16[704,256]{1,0:T(8,128)(2,1)}, u32[]{:S(2)}, u32[]{:S(2)}) collective-permute-start(bf16[704,256]{1,0:T(8,128)(2,1)} %collective-permute-done.21), channel_id=1, source_target_pairs={{0,4},{4,0},{8,12},{12,8},{16,20},{20,16},{24,28},{28,24},{1,5},{5... | collective-permute-start | bytes 1081352 | tf_op jit(solution)/shard_map/ppermute | solution.py:70
  146.4 21.4 %copy-start.14 = (f32[512]{0:T(512)S(1)}, f32[512]{0:T(512)}, u32[]{:S(2)}) copy-start(f32[512]{0:T(512)} %param.36) | copy-start | bytes 6148
  146.4 21.4 %copy-start.15 = (f32[512]{0:T(512)S(1)}, f32[512]{0:T(512)}, u32[]{:S(2)}) copy-start(f32[512]{0:T(512)} %param.35) | copy-start | bytes 6148
  148.3 30.0 %collective-permute-start.11 = (bf16[256,1408]{1,0:T(8,128)(2,1)}, bf16[256,1408]{1,0:T(8,128)(2,1)S(1)}, u32[]{:S(2)}, u32[]{:S(2)}) collective-permute-start(bf16[256,1408]{1,0:T(8,128)(2,1)} %collective-permute-done.10), channel_id=1, source_target_pairs={{0,4},{4,0},{8,12},{12,8},{16,20},{20,16},{24,28},{28,24},{1,5},{5... | collective-permute-start | bytes 2162696 | tf_op jit(solution)/shard_map/ppermute | solution.py:70
  149.1 44.6 %collective-permute-start.13 = (bf16[256,1408]{1,0:T(8,128)(2,1)}, bf16[256,1408]{1,0:T(8,128)(2,1)S(1)}, u32[]{:S(2)}, u32[]{:S(2)}) collective-permute-start(bf16[256,1408]{1,0:T(8,128)(2,1)} %collective-permute-done.12), channel_id=1, source_target_pairs={{0,4},{4,0},{8,12},{12,8},{16,20},{20,16},{24,28},{28,24},{1,5},{5... | collective-permute-start | bytes 2162696 | tf_op jit(solution)/shard_map/ppermute | solution.py:70
  150.3 57.2 %collective-permute-start.15 = (bf16[256,1408]{1,0:T(8,128)(2,1)}, bf16[256,1408]{1,0:T(8,128)(2,1)S(1)}, u32[]{:S(2)}, u32[]{:S(2)}) collective-permute-start(bf16[256,1408]{1,0:T(8,128)(2,1)} %collective-permute-done.14), channel_id=1, source_target_pairs={{0,4},{4,0},{8,12},{12,8},{16,20},{20,16},{24,28},{28,24},{1,5},{5... | collective-permute-start | bytes 2162696 | tf_op jit(solution)/shard_map/ppermute | solution.py:70
  155.1 6.4 %collective-permute-start.1 = (bf16[256,512]{1,0:T(8,128)(2,1)S(1)}, bf16[256,512]{1,0:T(8,128)(2,1)S(1)}, u32[]{:S(2)}, u32[]{:S(2)}) collective-permute-start(bf16[256,512]{1,0:T(8,128)(2,1)S(1)} %add_convert_fusion.2), channel_id=1, source_target_pairs={{0,2},{1,3},{2,0},{3,1},{4,6},{5,7},{6,4},{7,5},{8,10},{9,11},{10,... | collective-permute-start | bytes 786440 | tf_op jit(solution)/shard_map/ppermute | solution.py:70
  168.0 13.8 %collective-permute-start.5 = (bf16[256,512]{1,0:T(8,128)(2,1)S(1)}, bf16[256,512]{1,0:T(8,128)(2,1)S(1)}, u32[]{:S(2)}, u32[]{:S(2)}) collective-permute-start(bf16[256,512]{1,0:T(8,128)(2,1)S(1)} %add_convert_fusion.1), channel_id=1, source_target_pairs={{0,8},{4,12},{8,0},{12,4},{16,24},{20,28},{24,16},{28,20},{1,9},{5... | collective-permute-start | bytes 786440 | tf_op jit(solution)/shard_map/ppermute | solution.py:70
  179.2 16.0 %collective-permute-start.3 = (bf16[256,512]{1,0:T(8,128)(2,1)S(1)}, bf16[256,512]{1,0:T(8,128)(2,1)S(1)}, u32[]{:S(2)}, u32[]{:S(2)}) collective-permute-start(bf16[256,512]{1,0:T(8,128)(2,1)S(1)} %add_convert_fusion.1), channel_id=1, source_target_pairs={{0,2},{1,3},{2,0},{3,1},{4,6},{5,7},{6,4},{7,5},{8,10},{9,11},{10,... | collective-permute-start | bytes 786440 | tf_op jit(solution)/shard_map/ppermute | solution.py:70
  181.8 13.3 %collective-permute-start.7 = (bf16[256,512]{1,0:T(8,128)(2,1)S(1)}, bf16[256,512]{1,0:T(8,128)(2,1)S(1)}, u32[]{:S(2)}, u32[]{:S(2)}) collective-permute-start(bf16[256,512]{1,0:T(8,128)(2,1)S(1)} %collective-permute-done.5), channel_id=1, source_target_pairs={{0,2},{1,3},{2,0},{3,1},{4,6},{5,7},{6,4},{7,5},{8,10},{9,11},{10,... | collective-permute-start | bytes 786440 | tf_op jit(solution)/shard_map/ppermute | solution.py:70
  194.6 13.8 %collective-permute-start.2 = (bf16[256,512]{1,0:T(8,128)(2,1)S(1)}, bf16[256,512]{1,0:T(8,128)(2,1)S(1)}, u32[]{:S(2)}, u32[]{:S(2)}) collective-permute-start(bf16[256,512]{1,0:T(8,128)(2,1)S(1)} %add_convert_fusion.1), channel_id=1, source_target_pairs={{0,1},{1,0},{2,3},{3,2},{4,5},{5,4},{6,7},{7,6},{8,9},{9,8},{10,11... | collective-permute-start | bytes 786440 | tf_op jit(solution)/shard_map/ppermute | solution.py:70
  194.6 13.8 %collective-permute-start.6 = (bf16[256,512]{1,0:T(8,128)(2,1)S(1)}, bf16[256,512]{1,0:T(8,128)(2,1)S(1)}, u32[]{:S(2)}, u32[]{:S(2)}) collective-permute-start(bf16[256,512]{1,0:T(8,128)(2,1)S(1)} %collective-permute-done.5), channel_id=1, source_target_pairs={{0,1},{1,0},{2,3},{3,2},{4,5},{5,4},{6,7},{7,6},{8,9},{9,8},{10,11... | collective-permute-start | bytes 786440 | tf_op jit(solution)/shard_map/ppermute | solution.py:70
  195.1 13.3 %collective-permute-start.4 = (bf16[256,512]{1,0:T(8,128)(2,1)S(1)}, bf16[256,512]{1,0:T(8,128)(2,1)S(1)}, u32[]{:S(2)}, u32[]{:S(2)}) collective-permute-start(bf16[256,512]{1,0:T(8,128)(2,1)S(1)} %collective-permute-done.3), channel_id=1, source_target_pairs={{0,1},{1,0},{2,3},{3,2},{4,5},{5,4},{6,7},{7,6},{8,9},{9,8},{10,11... | collective-permute-start | bytes 786440 | tf_op jit(solution)/shard_map/ppermute | solution.py:70
  195.1 13.3 %collective-permute-start.8 = (bf16[256,512]{1,0:T(8,128)(2,1)S(1)}, bf16[256,512]{1,0:T(8,128)(2,1)S(1)}, u32[]{:S(2)}, u32[]{:S(2)}) collective-permute-start(bf16[256,512]{1,0:T(8,128)(2,1)S(1)} %collective-permute-done.7), channel_id=1, source_target_pairs={{0,1},{1,0},{2,3},{3,2},{4,5},{5,4},{6,7},{7,6},{8,9},{9,8},{10,11... | collective-permute-start | bytes 786440 | tf_op jit(solution)/shard_map/ppermute | solution.py:70
  214.5 1.8 copy-start.3
  217.6 2.7 %collective-permute-start.23 = (bf16[512,1024]{1,0:T(8,128)(2,1)S(1)}, bf16[512,1024]{1,0:T(8,128)(2,1)S(1)}, u32[]{:S(2)}, u32[]{:S(2)}) collective-permute-start(bf16[512,1024]{1,0:T(8,128)(2,1)S(1)} %pad_maximum_fusion), channel_id=1, source_target_pairs={{0,1},{1,0},{2,3},{3,2},{4,5},{5,4},{6,7},{7,6},{8,9},{9,8},{10,11... | collective-permute-start | bytes 3145736 | tf_op jit(solution)/shard_map/ppermute | solution.py:70
  221.6 34.3 %copy-start.16 = (f32[512]{0:T(512)S(1)}, f32[512]{0:T(512)}, u32[]{:S(2)}) copy-start(f32[512]{0:T(512)} %param.41) | copy-start | bytes 6148
  221.6 34.3 %copy-start.17 = (f32[512]{0:T(512)S(1)}, f32[512]{0:T(512)}, u32[]{:S(2)}) copy-start(f32[512]{0:T(512)} %param.40) | copy-start | bytes 6148
  221.7 20.1 %collective-permute-start.24 = (bf16[256,1024]{1,0:T(8,128)(2,1)S(1)}, bf16[256,1024]{1,0:T(8,128)(2,1)S(1)}, u32[]{:S(2)}, u32[]{:S(2)}) collective-permute-start(bf16[256,1024]{1,0:T(8,128)(2,1)S(1)} %pad_maximum_fusion.4), channel_id=1, source_target_pairs={{0,8},{4,12},{8,0},{12,4},{16,24},{20,28},{24,16},{28,20},{1,9},{5... | collective-permute-start | bytes 1572872 | tf_op jit(solution)/shard_map/ppermute | solution.py:70
  241.9 7.8 %collective-permute-start.25 = (bf16[256,512]{1,0:T(8,128)(2,1)S(1)}, bf16[256,512]{1,0:T(8,128)(2,1)S(1)}, u32[]{:S(2)}, u32[]{:S(2)}) collective-permute-start(bf16[256,512]{1,0:T(8,128)(2,1)S(1)} %fusion.56), channel_id=1, source_target_pairs={{0,2},{1,3},{2,0},{3,1},{4,6},{5,7},{6,4},{7,5},{8,10},{9,11},{10,... | collective-permute-start | bytes 786440 | tf_op jit(solution)/shard_map/ppermute | solution.py:70
Sparse Core Ops, SparseCore 0:
  10.2 99.5 all-gather.1

commit v2 on v1

--- a/solution.py
+++ b/solution.py
@@ -156,7 +156,13 @@
         :, 0, :
     ].astype(jnp.bfloat16)
     own_rows = jnp.concatenate([own_normed, own_rotated], axis=1)
-    all_rows = lax.all_gather(own_rows, ("sp", "tp"), axis=0, tiled=True)
+    all_rows = jnp.concatenate([own_rows, swap(own_rows, "sp", 1)], axis=0)
+    found = [all_rows]
+    for step in range(1, sp_count // 2):
+        found.append(swap(all_rows, "sp", step * 2))
+    all_rows = jnp.concatenate(found, axis=0)
+    for bit in reversed(tp_bits()):
+        all_rows = jnp.concatenate([all_rows, swap(all_rows, "tp", bit)], axis=0)
 
     half = gate_weight.shape[1] // 2
 
@@ -245,21 +251,26 @@
     both = jnp.dot(rows_in, gate_up, preferred_element_type=jnp.float32)
     hidden = (jax.nn.silu(both[:, :half]) * both[:, half:]).astype(jnp.bfloat16)
     down = place(down_blocks, 1, (half, width_total))
+    bits = tp_bits()
+
+    def feed_half(rows):
+        made = {
+            q: jnp.dot(
+                rows,
+                down[:, q * feature_width : (q + 1) * feature_width],
+                preferred_element_type=jnp.float32,
+            )
+            for q in range(tp_count)
+        }
+        return fold_tp(made, bits[:-1])
+
+    mate_terms = feed_half(hidden[row_count:])
+    kept = sorted(mate_terms)
+    packed = jnp.concatenate([mate_terms[q].astype(jnp.bfloat16) for q in kept], axis=1)
+    got = swap(packed, "sp", 2)
+    own_terms = feed_half(hidden[:row_count])
     feed_terms = {
-        q: jnp.dot(
-            hidden,
-            down[:, q * feature_width : (q + 1) * feature_width],
-            preferred_element_type=jnp.float32,
-        )
-        for q in range(tp_count)
-    }
-    bits = tp_bits()
-    feed_terms = fold_tp(feed_terms, bits[:-1])
-    kept = sorted(feed_terms)
-    packed = jnp.concatenate([feed_terms[q][row_count:].astype(jnp.bfloat16) for q in kept], axis=1)
-    got = swap(packed, "sp", 2)
-    feed_terms = {
-        q: feed_terms[q][:row_count]
+        q: own_terms[q]
         + got[:, n * feature_width : (n + 1) * feature_width].astype(jnp.float32)
         for n, q in enumerate(kept)
     }

time: 265 us -> 243 us (0.917)
  waiting for transfers between devices: 123 us -> 106 us
  between operations: 13.9 us -> 0.61 us
  local copies, waits for them, and re-layouts: 28.1 us -> 38.5 us
    all_gather x1 -> x0, waiting for transfers between devices: 31.9 us -> none  [body(): all_rows = lax.all_gather(own_rows, ('sp', 'tp'), axis=0, tiled=True)]
    ppermute x26 -> x33, waiting for transfers between devices: 91.4 us -> 106 us  [swap(): return lax.ppermute(value, axis, [(i, i ^ bit) for i in range(count)])]
    concatenate x0 -> x3, local copies, waits for them, and re-layouts: none -> 6.08 us  [the longest x2 4.25 us: body(): all_rows = jnp.concatenate([all_rows, swap(all_rows, 'tp', bit)], axis=0)]
    ppermute x26 -> x33, starting transfers between devices: 43.6 us -> 44.6 us  [swap(): return lax.ppermute(value, axis, [(i, i ^ bit) for i in range(count)])]
  transfers between devices with their start and end apart: 27 -> 33, of which waited for: 13 -> 14; matrix products, arithmetic and copies ran while one was open for 21% -> 24% of each run, Pallas kernels for 0% -> 0%
where the time goes in v2:
time: 243 us; the launch traced here: 241 us
  waiting for transfers between devices  106 us (44%)
  starting transfers between devices  44.6 us (18%)
  local copies, waits for them, and re-layouts  38.5 us (16%)
  matrix products  27.6 us (11%)
  other arithmetic  12.2 us (5%)
  blocking collectives  11.9 us (5%)
    ppermute x33, waiting for transfers between devices, swap(): return lax.ppermute(value, axis, [(i, i ^ bit) for i in range(count)])  106 us
    ppermute x33, starting transfers between devices, swap(): return lax.ppermute(value, axis, [(i, i ^ bit) for i in range(count)])  44.6 us
    dynamic_update_slice x15, local copies, waits for them, and re-layouts, place(): whole = lax.dynamic_update_slice_in_dim(whole, block, at, axis)  20.6 us
    psum x2, blocking collectives, layer_stats(): total = lax.psum(stats, 'tp')  11.9 us
    dot_general x1, matrix products, body(): both = jnp.dot(rows_in, gate_up, preferred_element_type=jnp.float32)  6.08 us
  transfers between devices with their start and end apart: 33, of which 14 were waited for; matrix products, arithmetic and copies ran while one was open for 24% of the time, Pallas kernels for 0%

profile of v2, /device:TPU:0, one launch (start us, length us, event | category | flops | bytes accessed | tf_op | source)
XLA Modules:
  0.0 241.4 jit_solution(4098026636169173075)
XLA Ops:
  0.0 2.9 %constant_dynamic-slice_fusion.2 = (bf16[256,704]{1,0:T(8,128)(2,1)S(1)}, bf16[256,704]{1,0:T(8,128)(2,1)S(1)}, bf16[256,704]{1,0:T(8,128)(2,1)S(1)}, bf16[256,704]{1,0:T(8,128)(2,1)}) fusion(bf16[256,1408]{1,0:T(8,128)(2,1)} %param.38, u32[]{:T(128)S(6)} %mul.477, u32[]{:T(128)S(6)} %mul.472, bf16[256,1408]{1,0:T(8,128)(2,1)} %param.37), kind=kLoop, calls=%fused_computation.194 | loop fusion | bytes 2883592 | tf_op jit(solution)/shard_map/dynamic_slice | solution.py:171
  2.9 2.9 %broadcast_in_dim.11 = bf16[2048,1408]{1,0:T(8,128)(2,1)} broadcast(bf16[]{:T(256)} %constant.128.clone.1), dimensions={} | broadcast | bytes 5767170 | tf_op jit(solution)/shard_map/broadcast_in_dim | solution.py:193
  7.2 3.0 %collective-permute-start.15 = (bf16[256,1408]{1,0:T(8,128)(2,1)}, bf16[256,1408]{1,0:T(8,128)(2,1)}, u32[]{:S(2)}, u32[]{:S(2)}) collective-permute-start(bf16[256,1408]{1,0:T(8,128)(2,1)} %get-tuple-element.11), channel_id=1, source_target_pairs={{0,4},{4,0},{8,12},{12,8},{16,20},{20,16},{24,28},{28,24},{1,5},{5... | collective-permute-start | bytes 2162696 | tf_op jit(solution)/shard_map/ppermute | solution.py:70
  10.2 2.6 %collective-permute-start.18 = (bf16[256,1408]{1,0:T(8,128)(2,1)}, bf16[256,1408]{1,0:T(8,128)(2,1)}, u32[]{:S(2)}, u32[]{:S(2)}) collective-permute-start(bf16[256,1408]{1,0:T(8,128)(2,1)} %get-tuple-element.11), channel_id=1, source_target_pairs={{0,16},{4,20},{8,24},{12,28},{16,0},{20,4},{24,8},{28,12},{1,17},{... | collective-permute-start | bytes 2162696 | tf_op jit(solution)/shard_map/ppermute | solution.py:70
  16.5 2.0 constant_dynamic-update-slice_fusion.7
  19.5 8.5 %collective-permute-done = bf16[64,288]{0,1:T(8,128)(2,1)S(1)} collective-permute-done((bf16[64,288]{0,1:T(8,128)(2,1)}, bf16[64,288]{0,1:T(8,128)(2,1)S(1)}, u32[]{:S(2)}, u32[]{:S(2)}) %collective-permute-start) | collective-permute-done | bytes 36896 | tf_op jit(solution)/shard_map/ppermute | solution.py:70
  29.0 1.9 collective-permute-start.1
  30.9 2.6 %collective-permute-start.2 = (bf16[128,288]{0,1:T(8,128)(2,1)S(1)}, bf16[128,288]{0,1:T(8,128)(2,1)}, u32[]{:S(2)}, u32[]{:S(2)}) collective-permute-start(bf16[128,288]{0,1:T(8,128)(2,1)S(1)} %pad_maximum_fusion.8), channel_id=1, source_target_pairs={{0,16},{4,20},{8,24},{12,28},{16,0},{20,4},{24,8},{28,12},{1,17},{... | collective-permute-start | bytes 221192 | tf_op jit(solution)/shard_map/ppermute | solution.py:70
  33.5 1.9 convolution_bitcast_fusion.5
  36.7 1.6 collective-permute-start.22
  38.3 11.8 %collective-permute-done.2 = bf16[128,288]{0,1:T(8,128)(2,1)} collective-permute-done((bf16[128,288]{0,1:T(8,128)(2,1)S(1)}, bf16[128,288]{0,1:T(8,128)(2,1)}, u32[]{:S(2)}, u32[]{:S(2)}) %collective-permute-start.2) | collective-permute-done | bytes 73760 | tf_op jit(solution)/shard_map/ppermute | solution.py:70
  50.0 1.8 concatenate.84
  53.4 2.1 pad_maximum_fusion.1
  55.5 5.1 %collective-permute-done.4 = bf16[512,288]{0,1:T(8,128)(2,1)} collective-permute-done((bf16[512,288]{0,1:T(8,128)(2,1)}, bf16[512,288]{0,1:T(8,128)(2,1)}, u32[]{:S(2)}, u32[]{:S(2)}) %collective-permute-start.4) | collective-permute-done | bytes 294944 | tf_op jit(solution)/shard_map/ppermute | solution.py:70
  60.6 2.0 concatenate.85
  63.6 1.9 constant_dynamic-update-slice_fusion.16
  65.4 1.9 collective-permute-start.16
  68.3 3.5 %collective-permute-start.20 = (bf16[256,1408]{1,0:T(8,128)(2,1)}, bf16[256,1408]{1,0:T(8,128)(2,1)}, u32[]{:S(2)}, u32[]{:S(2)}) collective-permute-start(bf16[256,1408]{1,0:T(8,128)(2,1)} %pad_maximum_fusion.1), channel_id=1, source_target_pairs={{0,24},{4,28},{8,16},{12,20},{16,8},{20,12},{24,0},{28,4},{1,25},{... | collective-permute-start | bytes 2162696 | tf_op jit(solution)/shard_map/ppermute | solution.py:70
  74.5 2.3 concatenate.86
  76.9 2.3 convolution_bitcast_fusion.3
  79.2 2.2 convolution_bitcast_fusion.1
  81.4 2.1 fusion.169
  85.0 2.1 fusion.168
  88.1 1.8 fusion.38
  92.6 25.8 %collective-permute-done.25 = bf16[704,256]{1,0:T(8,128)(2,1)} collective-permute-done((bf16[704,256]{1,0:T(8,128)(2,1)}, bf16[704,256]{1,0:T(8,128)(2,1)}, u32[]{:S(2)}, u32[]{:S(2)}) %collective-permute-start.25) | collective-permute-done | bytes 360480 | tf_op jit(solution)/shard_map/ppermute | solution.py:70
  118.4 2.6 %collective-permute-start.27 = (bf16[704,256]{1,0:T(8,128)(2,1)}, bf16[704,256]{1,0:T(8,128)(2,1)S(1)}, u32[]{:S(2)}, u32[]{:S(2)}) collective-permute-start(bf16[704,256]{1,0:T(8,128)(2,1)} %get-tuple-element.18), channel_id=1, source_target_pairs={{0,24},{4,28},{8,16},{12,20},{16,8},{20,12},{24,0},{28,4},{1,25},{... | collective-permute-start | bytes 1081352 | tf_op jit(solution)/shard_map/ppermute | solution.py:70
  121.6 2.1 constant_dynamic-update-slice_fusion.14
  123.7 2.1 constant_dynamic-update-slice_fusion.13
  125.7 5.1 %collective-permute-done.27 = bf16[704,256]{1,0:T(8,128)(2,1)S(1)} collective-permute-done((bf16[704,256]{1,0:T(8,128)(2,1)}, bf16[704,256]{1,0:T(8,128)(2,1)S(1)}, u32[]{:S(2)}, u32[]{:S(2)}) %collective-permute-start.27) | collective-permute-done | bytes 360480 | tf_op jit(solution)/shard_map/ppermute | solution.py:70
  136.8 5.5 %collective-permute-done.26 = bf16[704,256]{1,0:T(8,128)(2,1)S(1)} collective-permute-done((bf16[704,256]{1,0:T(8,128)(2,1)}, bf16[704,256]{1,0:T(8,128)(2,1)S(1)}, u32[]{:S(2)}, u32[]{:S(2)}) %collective-permute-start.26) | collective-permute-done | bytes 360480 | tf_op jit(solution)/shard_map/ppermute | solution.py:70
  144.1 4.5 %collective-permute-done.7 = bf16[256,512]{1,0:T(8,128)(2,1)S(1)} collective-permute-done((bf16[256,512]{1,0:T(8,128)(2,1)S(1)}, bf16[256,512]{1,0:T(8,128)(2,1)S(1)}, u32[]{:S(2)}, u32[]{:S(2)}) %collective-permute-start.7) | collective-permute-done | bytes 262176 | tf_op jit(solution)/shard_map/ppermute | solution.py:70
  149.6 6.2 %psum.14 = f32[2,256]{1,0:T(2,128)S(1)} all-reduce(f32[2,256]{1,0:T(2,128)S(1)} %pad_maximum_fusion.9), channel_id=1, replica_groups=mesh['sp'=8,'tp'=4] {'tp'}, use_global_device_ids=true, to_apply=%region_8.9 | all-reduce | flops 512 | bytes 4096 | tf_op jit(solution)/shard_map/psum | solution.py:106
  157.1 5.4 %collective-permute-start.11 = (bf16[256,512]{1,0:T(8,128)(2,1)S(1)}, bf16[256,512]{1,0:T(8,128)(2,1)S(1)}, u32[]{:S(2)}, u32[]{:S(2)}) collective-permute-start(bf16[256,512]{1,0:T(8,128)(2,1)S(1)} %add_convert_fusion.1), channel_id=1, source_target_pairs={{0,8},{4,12},{8,0},{12,4},{16,24},{20,28},{24,16},{28,20},{1,9},{5... | collective-permute-start | bytes 786440 | tf_op jit(solution)/shard_map/ppermute | solution.py:70
  163.6 2.0 collective-permute-done.17
  165.6 2.0 constant_dynamic-update-slice_fusion.12
  170.0 2.0 constant_dynamic-update-slice_fusion.11
  172.0 9.0 %collective-permute-done.19 = bf16[256,1408]{1,0:T(8,128)(2,1)} collective-permute-done((bf16[256,1408]{1,0:T(8,128)(2,1)}, bf16[256,1408]{1,0:T(8,128)(2,1)}, u32[]{:S(2)}, u32[]{:S(2)}) %collective-permute-start.19) | collective-permute-done | bytes 720928 | tf_op jit(solution)/shard_map/ppermute | solution.py:70
  181.0 2.0 constant_dynamic-update-slice_fusion.10
  184.1 2.0 constant_dynamic-update-slice_fusion.9
  186.1 8.4 %collective-permute-done.21 = bf16[256,1408]{1,0:T(8,128)(2,1)} collective-permute-done((bf16[256,1408]{1,0:T(8,128)(2,1)}, bf16[256,1408]{1,0:T(8,128)(2,1)}, u32[]{:S(2)}, u32[]{:S(2)}) %collective-permute-start.21) | collective-permute-done | bytes 720928 | tf_op jit(solution)/shard_map/ppermute | solution.py:70
  194.6 2.0 constant_dynamic-update-slice_fusion.8
  196.6 6.1 %fusion.4 = f32[512,1408]{1,0:T(8,128)S(1)} fusion(bf16[2048,1408]{1,0:T(8,128)(2,1)} %constant_dynamic-update-slice_fusion.8, bf16[256,512]{1,0:T(8,128)(2,1)S(1)} %collective-permute-done.14, bf16[256,512]{1,0:T(8,128)(2,1)S(1)} %collective-permute-done.13, bf16[256,512]{1,0:T(8,128)(2,1)S(1)} %collective-permute-done.12, ...), kind=kOutput, calls=%fused_computation.12 | convolution fusion | flops 2969567232 | bytes 10747904 | tf_op jit(solution)/shard_map/dot_general | solution.py:251
  206.9 5.2 %collective-permute-start.31 = (bf16[256,1024]{1,0:T(8,128)(2,1)S(1)}, bf16[256,1024]{1,0:T(8,128)(2,1)S(1)}, u32[]{:S(2)}, u32[]{:S(2)}) collective-permute-start(bf16[256,1024]{1,0:T(8,128)(2,1)S(1)} %pad_maximum_fusion.5), channel_id=1, source_target_pairs={{0,8},{4,12},{8,0},{12,4},{16,24},{20,28},{24,16},{28,20},{1,9},{5... | collective-permute-start | bytes 1572872 | tf_op jit(solution)/shard_map/ppermute | solution.py:70
  212.0 12.2 %collective-permute-done.31 = bf16[256,1024]{1,0:T(8,128)(2,1)S(1)} collective-permute-done((bf16[256,1024]{1,0:T(8,128)(2,1)S(1)}, bf16[256,1024]{1,0:T(8,128)(2,1)S(1)}, u32[]{:S(2)}, u32[]{:S(2)}) %collective-permute-start.31) | collective-permute-done | bytes 524320 | tf_op jit(solution)/shard_map/ppermute | solution.py:70
  224.7 1.6 collective-permute-start.32
  226.3 6.2 %collective-permute-done.32 = bf16[256,512]{1,0:T(8,128)(2,1)S(1)} collective-permute-done((bf16[256,512]{1,0:T(8,128)(2,1)S(1)}, bf16[256,512]{1,0:T(8,128)(2,1)S(1)}, u32[]{:S(2)}, u32[]{:S(2)}) %collective-permute-start.32) | collective-permute-done | bytes 262176 | tf_op jit(solution)/shard_map/ppermute | solution.py:70
  233.8 5.7 %psum.15 = f32[2,256]{1,0:T(2,128)S(1)} all-reduce(f32[2,256]{1,0:T(2,128)S(1)} %pad_maximum_fusion.10), channel_id=1, replica_groups=mesh['sp'=8,'tp'=4] {'tp'}, use_global_device_ids=true, to_apply=%region_11.12 | all-reduce | flops 512 | bytes 4096 | tf_op jit(solution)/shard_map/psum | solution.py:106
  239.5 1.9 add_convert_fusion
  (144 shorter events, 40.1 us)
Async XLA Ops:
  0.0 18.6 %copy-start = (bf16[512,160]{0,1:T(8,128)(2,1)S(1)}, bf16[512,160]{0,1:T(8,128)(2,1)}, u32[]{:S(2)}) copy-start(bf16[512,160]{0,1:T(8,128)(2,1)} %param.30) | copy-start | bytes 491524
  2.9 9.8 %copy-start.15 = (bf16[256,32]{0,1:T(8,128)(2,1)S(1)}, bf16[256,32]{0,1:T(8,128)(2,1)}, u32[]{:S(2)}) copy-start(bf16[256,32]{0,1:T(8,128)(2,1)} %param.24) | copy-start | bytes 49156
  2.9 10.9 %copy-start.21 = (f32[256]{0:T(256)S(1)}, f32[256]{0:T(256)}, u32[]{:S(2)}) copy-start(f32[256]{0:T(256)} %param.26) | copy-start | bytes 3076
  2.9 12.3 %copy-start.6 = (bf16[256,512]{1,0:T(8,128)(2,1)S(1)}, bf16[256,512]{1,0:T(8,128)(2,1)}, u32[]{:S(2)}) copy-start(bf16[256,512]{1,0:T(8,128)(2,1)} %param.22) | copy-start | bytes 786436
  5.8 9.6 %copy-start.5 = (bf16[64,2048]{1,0:T(8,128)(2,1)S(1)}, bf16[64,2048]{1,0:T(8,128)(2,1)}, u32[]{:S(2)}) copy-start(bf16[64,2048]{1,0:T(8,128)(2,1)} %param.33) | copy-start | bytes 786436
  7.2 113.9 %collective-permute-start.15 = (bf16[256,1408]{1,0:T(8,128)(2,1)}, bf16[256,1408]{1,0:T(8,128)(2,1)}, u32[]{:S(2)}, u32[]{:S(2)}) collective-permute-start(bf16[256,1408]{1,0:T(8,128)(2,1)} %get-tuple-element.11), channel_id=1, source_target_pairs={{0,4},{4,0},{8,12},{12,8},{16,20},{20,16},{24,28},{28,24},{1,5},{5... | collective-permute-start | bytes 2162696 | tf_op jit(solution)/shard_map/ppermute | solution.py:70
  10.2 123.8 %collective-permute-start.18 = (bf16[256,1408]{1,0:T(8,128)(2,1)}, bf16[256,1408]{1,0:T(8,128)(2,1)}, u32[]{:S(2)}, u32[]{:S(2)}) collective-permute-start(bf16[256,1408]{1,0:T(8,128)(2,1)} %get-tuple-element.11), channel_id=1, source_target_pairs={{0,16},{4,20},{8,24},{12,28},{16,0},{20,4},{24,8},{28,12},{1,17},{... | collective-permute-start | bytes 2162696 | tf_op jit(solution)/shard_map/ppermute | solution.py:70
  14.7 13.3 %collective-permute-start = (bf16[64,288]{0,1:T(8,128)(2,1)}, bf16[64,288]{0,1:T(8,128)(2,1)S(1)}, u32[]{:S(2)}, u32[]{:S(2)}) collective-permute-start(bf16[64,288]{0,1:T(8,128)(2,1)} %pad_maximum_fusion.7), channel_id=1, source_target_pairs={{0,4},{4,0},{8,12},{12,8},{16,20},{20,16},{24,28},{28,24},{1,5},{5... | collective-permute-start | bytes 110600 | tf_op jit(solution)/shard_map/ppermute | solution.py:70
  29.0 7.6 %collective-permute-start.1 = (bf16[128,288]{0,1:T(8,128)(2,1)S(1)}, bf16[128,288]{0,1:T(8,128)(2,1)}, u32[]{:S(2)}, u32[]{:S(2)}) collective-permute-start(bf16[128,288]{0,1:T(8,128)(2,1)S(1)} %pad_maximum_fusion.8), channel_id=1, source_target_pairs={{0,8},{4,12},{8,0},{12,4},{16,24},{20,28},{24,16},{28,20},{1,9},{5... | collective-permute-start | bytes 221192 | tf_op jit(solution)/shard_map/ppermute | solution.py:70
  30.9 19.1 %collective-permute-start.2 = (bf16[128,288]{0,1:T(8,128)(2,1)S(1)}, bf16[128,288]{0,1:T(8,128)(2,1)}, u32[]{:S(2)}, u32[]{:S(2)}) collective-permute-start(bf16[128,288]{0,1:T(8,128)(2,1)S(1)} %pad_maximum_fusion.8), channel_id=1, source_target_pairs={{0,16},{4,20},{8,24},{12,28},{16,0},{20,4},{24,8},{28,12},{1,17},{... | collective-permute-start | bytes 221192 | tf_op jit(solution)/shard_map/ppermute | solution.py:70
  33.5 16.6 %collective-permute-start.3 = (bf16[128,288]{0,1:T(8,128)(2,1)S(1)}, bf16[128,288]{0,1:T(8,128)(2,1)}, u32[]{:S(2)}, u32[]{:S(2)}) collective-permute-start(bf16[128,288]{0,1:T(8,128)(2,1)S(1)} %pad_maximum_fusion.8), channel_id=1, source_target_pairs={{0,24},{4,28},{8,16},{12,20},{16,8},{20,12},{24,0},{28,4},{1,25},{... | collective-permute-start | bytes 221192 | tf_op jit(solution)/shard_map/ppermute | solution.py:70
  36.7 28.8 %collective-permute-start.22 = (bf16[704,256]{1,0:T(8,128)(2,1)}, bf16[704,256]{1,0:T(8,128)(2,1)}, u32[]{:S(2)}, u32[]{:S(2)}) collective-permute-start(bf16[704,256]{1,0:T(8,128)(2,1)} %get-tuple-element.13), channel_id=1, source_target_pairs={{0,4},{4,0},{8,12},{12,8},{16,20},{20,16},{24,28},{28,24},{1,5},{5... | collective-permute-start | bytes 1081352 | tf_op jit(solution)/shard_map/ppermute | solution.py:70
  50.0 18.3 %collective-permute-start.23 = (bf16[704,256]{1,0:T(8,128)(2,1)}, bf16[704,256]{1,0:T(8,128)(2,1)}, u32[]{:S(2)}, u32[]{:S(2)}) collective-permute-start(bf16[704,256]{1,0:T(8,128)(2,1)} %get-tuple-element.18), channel_id=1, source_target_pairs={{0,8},{4,12},{8,0},{12,4},{16,24},{20,28},{24,16},{28,20},{1,9},{5... | collective-permute-start | bytes 1081352 | tf_op jit(solution)/shard_map/ppermute | solution.py:70
  51.9 8.7 %collective-permute-start.4 = (bf16[512,288]{0,1:T(8,128)(2,1)}, bf16[512,288]{0,1:T(8,128)(2,1)}, u32[]{:S(2)}, u32[]{:S(2)}) collective-permute-start(bf16[512,288]{0,1:T(8,128)(2,1)} %concatenate.84), channel_id=1, source_target_pairs={{0,2},{1,3},{2,0},{3,1},{4,6},{5,7},{6,4},{7,5},{8,10},{9,11},{10,... | collective-permute-start | bytes 884744 | tf_op jit(solution)/shard_map/ppermute | solution.py:70
  55.5 21.3 %copy-start.10 = (f32[256,1,96]{0,2,1:T(8,128)S(1)}, f32[256,1,96]{0,2,1:T(8,128)}, u32[]{:S(2)}) copy-start(f32[256,1,96]{0,2,1:T(8,128)} %convolution_bitcast_fusion.5) | copy-start | bytes 294916
  55.5 21.4 %copy-start.12 = (bf16[256,64]{0,1:T(8,128)(2,1)S(1)}, bf16[256,64]{0,1:T(8,128)(2,1)}, u32[]{:S(2)}) copy-start(bf16[256,64]{0,1:T(8,128)(2,1)} %param.28) | copy-start | bytes 98308
  62.5 10.4 %collective-permute-start.5 = (bf16[1024,288]{0,1:T(8,128)(2,1)}, bf16[1024,288]{0,1:T(8,128)(2,1)}, u32[]{:S(2)}, u32[]{:S(2)}) collective-permute-start(bf16[1024,288]{0,1:T(8,128)(2,1)} %concatenate.85), channel_id=1, source_target_pairs={{0,1},{1,0},{2,3},{3,2},{4,5},{5,4},{6,7},{7,6},{8,9},{9,8},{10,11... | collective-permute-start | bytes 1769480 | tf_op jit(solution)/shard_map/ppermute | solution.py:70
  65.4 56.2 %collective-permute-start.16 = (bf16[256,1408]{1,0:T(8,128)(2,1)}, bf16[256,1408]{1,0:T(8,128)(2,1)}, u32[]{:S(2)}, u32[]{:S(2)}) collective-permute-start(bf16[256,1408]{1,0:T(8,128)(2,1)} %pad_maximum_fusion.1), channel_id=1, source_target_pairs={{0,8},{4,12},{8,0},{12,4},{16,24},{20,28},{24,16},{28,20},{1,9},{5... | collective-permute-start | bytes 2162696 | tf_op jit(solution)/shard_map/ppermute | solution.py:70
  68.3 66.2 %collective-permute-start.20 = (bf16[256,1408]{1,0:T(8,128)(2,1)}, bf16[256,1408]{1,0:T(8,128)(2,1)}, u32[]{:S(2)}, u32[]{:S(2)}) collective-permute-start(bf16[256,1408]{1,0:T(8,128)(2,1)} %pad_maximum_fusion.1), channel_id=1, source_target_pairs={{0,24},{4,28},{8,16},{12,20},{16,8},{20,12},{24,0},{28,4},{1,25},{... | collective-permute-start | bytes 2162696 | tf_op jit(solution)/shard_map/ppermute | solution.py:70
  72.9 6.3 %copy-start.9 = (f32[256,1,160]{0,2,1:T(8,128)S(1)}, f32[256,1,160]{0,2,1:T(8,128)}, u32[]{:S(2)}) copy-start(f32[256,1,160]{0,2,1:T(8,128)} %convolution_bitcast_fusion.4) | copy-start | bytes 491524
  74.5 43.9 %collective-permute-start.25 = (bf16[704,256]{1,0:T(8,128)(2,1)}, bf16[704,256]{1,0:T(8,128)(2,1)}, u32[]{:S(2)}, u32[]{:S(2)}) collective-permute-start(bf16[704,256]{1,0:T(8,128)(2,1)} %get-tuple-element.13), channel_id=1, source_target_pairs={{0,16},{4,20},{8,24},{12,28},{16,0},{20,4},{24,8},{28,12},{1,17},{... | collective-permute-start | bytes 1081352 | tf_op jit(solution)/shard_map/ppermute | solution.py:70
  90.0 42.8 %copy-start.2 = (bf16[704,2048]{1,0:T(8,128)(2,1)S(1)}, bf16[704,2048]{1,0:T(8,128)(2,1)}, u32[]{:S(2)}) copy-start(bf16[704,2048]{1,0:T(8,128)(2,1)} %copy-done.1) | copy-start | bytes 8650756
  91.3 45.2 %copy-start.3 = (bf16[192,2048]{1,0:T(8,128)(2,1)S(1)}, bf16[192,2048]{1,0:T(8,128)(2,1)}, u32[]{:S(2)}) copy-start(bf16[192,2048]{1,0:T(8,128)(2,1)} %constant_dynamic-update-slice_fusion.16) | copy-start | bytes 2359300
  118.4 12.4 %collective-permute-start.27 = (bf16[704,256]{1,0:T(8,128)(2,1)}, bf16[704,256]{1,0:T(8,128)(2,1)S(1)}, u32[]{:S(2)}, u32[]{:S(2)}) collective-permute-start(bf16[704,256]{1,0:T(8,128)(2,1)} %get-tuple-element.18), channel_id=1, source_target_pairs={{0,24},{4,28},{8,16},{12,20},{16,8},{20,12},{24,0},{28,4},{1,25},{... | collective-permute-start | bytes 1081352 | tf_op jit(solution)/shard_map/ppermute | solution.py:70
  121.1 10.2 %collective-permute-start.24 = (bf16[704,256]{1,0:T(8,128)(2,1)}, bf16[704,256]{1,0:T(8,128)(2,1)S(1)}, u32[]{:S(2)}, u32[]{:S(2)}) collective-permute-start(bf16[704,256]{1,0:T(8,128)(2,1)} %collective-permute-done.23), channel_id=1, source_target_pairs={{0,4},{4,0},{8,12},{12,8},{16,20},{20,16},{24,28},{28,24},{1,5},{5... | collective-permute-start | bytes 1081352 | tf_op jit(solution)/shard_map/ppermute | solution.py:70
  121.6 14.5 %collective-permute-start.6 = (bf16[256,1024]{1,0:T(8,128)(2,1)S(1)}, bf16[256,1024]{1,0:T(8,128)(2,1)S(1)}, u32[]{:S(2)}, u32[]{:S(2)}) collective-permute-start(bf16[256,1024]{1,0:T(8,128)(2,1)S(1)} %pad_maximum_fusion.2), channel_id=1, source_target_pairs={{0,1},{1,0},{2,3},{3,2},{4,5},{5,4},{6,7},{7,6},{8,9},{9,8},{10,11... | collective-permute-start | bytes 1572872 | tf_op jit(solution)/shard_map/ppermute | solution.py:70
  123.7 25.0 %copy-start.8 = (bf16[256,512]{1,0:T(8,128)(2,1)S(1)}, bf16[256,512]{1,0:T(8,128)(2,1)}, u32[]{:S(2)}) copy-start(bf16[256,512]{1,0:T(8,128)(2,1)} %param.21) | copy-start | bytes 786436
  130.8 11.5 %collective-permute-start.26 = (bf16[704,256]{1,0:T(8,128)(2,1)}, bf16[704,256]{1,0:T(8,128)(2,1)S(1)}, u32[]{:S(2)}, u32[]{:S(2)}) collective-permute-start(bf16[704,256]{1,0:T(8,128)(2,1)} %collective-permute-done.25), channel_id=1, source_target_pairs={{0,4},{4,0},{8,12},{12,8},{16,20},{20,16},{24,28},{28,24},{1,5},{5... | collective-permute-start | bytes 1081352 | tf_op jit(solution)/shard_map/ppermute | solution.py:70
  131.3 31.2 %collective-permute-start.28 = (bf16[704,256]{1,0:T(8,128)(2,1)S(1)}, bf16[704,256]{1,0:T(8,128)(2,1)}, u32[]{:S(2)}, u32[]{:S(2)}) collective-permute-start(bf16[704,256]{1,0:T(8,128)(2,1)S(1)} %collective-permute-done.27), channel_id=1, source_target_pairs={{0,4},{4,0},{8,12},{12,8},{16,20},{20,16},{24,28},{28,24},{1,5},{5... | collective-permute-start | bytes 1081352 | tf_op jit(solution)/shard_map/ppermute | solution.py:70
  132.9 23.0 %copy-start.16 = (f32[512]{0:T(512)S(1)}, f32[512]{0:T(512)}, u32[]{:S(2)}) copy-start(f32[512]{0:T(512)} %param.36) | copy-start | bytes 6148
  132.9 23.0 %copy-start.17 = (f32[512]{0:T(512)S(1)}, f32[512]{0:T(512)}, u32[]{:S(2)}) copy-start(f32[512]{0:T(512)} %param.35) | copy-start | bytes 6148
  133.9 31.6 %collective-permute-start.17 = (bf16[256,1408]{1,0:T(8,128)(2,1)}, bf16[256,1408]{1,0:T(8,128)(2,1)}, u32[]{:S(2)}, u32[]{:S(2)}) collective-permute-start(bf16[256,1408]{1,0:T(8,128)(2,1)} %collective-permute-done.16), channel_id=1, source_target_pairs={{0,4},{4,0},{8,12},{12,8},{16,20},{20,16},{24,28},{28,24},{1,5},{5... | collective-permute-start | bytes 2162696 | tf_op jit(solution)/shard_map/ppermute | solution.py:70
  134.5 46.5 %collective-permute-start.19 = (bf16[256,1408]{1,0:T(8,128)(2,1)}, bf16[256,1408]{1,0:T(8,128)(2,1)}, u32[]{:S(2)}, u32[]{:S(2)}) collective-permute-start(bf16[256,1408]{1,0:T(8,128)(2,1)} %collective-permute-done.18), channel_id=1, source_target_pairs={{0,4},{4,0},{8,12},{12,8},{16,20},{20,16},{24,28},{28,24},{1,5},{5... | collective-permute-start | bytes 2162696 | tf_op jit(solution)/shard_map/ppermute | solution.py:70
  136.0 58.5 %collective-permute-start.21 = (bf16[256,1408]{1,0:T(8,128)(2,1)}, bf16[256,1408]{1,0:T(8,128)(2,1)}, u32[]{:S(2)}, u32[]{:S(2)}) collective-permute-start(bf16[256,1408]{1,0:T(8,128)(2,1)} %collective-permute-done.20), channel_id=1, source_target_pairs={{0,4},{4,0},{8,12},{12,8},{16,20},{20,16},{24,28},{28,24},{1,5},{5... | collective-permute-start | bytes 2162696 | tf_op jit(solution)/shard_map/ppermute | solution.py:70
  142.3 6.4 %collective-permute-start.7 = (bf16[256,512]{1,0:T(8,128)(2,1)S(1)}, bf16[256,512]{1,0:T(8,128)(2,1)S(1)}, u32[]{:S(2)}, u32[]{:S(2)}) collective-permute-start(bf16[256,512]{1,0:T(8,128)(2,1)S(1)} %add_convert_fusion.2), channel_id=1, source_target_pairs={{0,2},{1,3},{2,0},{3,1},{4,6},{5,7},{6,4},{7,5},{8,10},{9,11},{10,... | collective-permute-start | bytes 786440 | tf_op jit(solution)/shard_map/ppermute | solution.py:70
  157.1 12.0 %collective-permute-start.11 = (bf16[256,512]{1,0:T(8,128)(2,1)S(1)}, bf16[256,512]{1,0:T(8,128)(2,1)S(1)}, u32[]{:S(2)}, u32[]{:S(2)}) collective-permute-start(bf16[256,512]{1,0:T(8,128)(2,1)S(1)} %add_convert_fusion.1), channel_id=1, source_target_pairs={{0,8},{4,12},{8,0},{12,4},{16,24},{20,28},{24,16},{28,20},{1,9},{5... | collective-permute-start | bytes 786440 | tf_op jit(solution)/shard_map/ppermute | solution.py:70
  167.6 16.0 %collective-permute-start.9 = (bf16[256,512]{1,0:T(8,128)(2,1)S(1)}, bf16[256,512]{1,0:T(8,128)(2,1)S(1)}, u32[]{:S(2)}, u32[]{:S(2)}) collective-permute-start(bf16[256,512]{1,0:T(8,128)(2,1)S(1)} %add_convert_fusion.1), channel_id=1, source_target_pairs={{0,2},{1,3},{2,0},{3,1},{4,6},{5,7},{6,4},{7,5},{8,10},{9,11},{10,... | collective-permute-start | bytes 786440 | tf_op jit(solution)/shard_map/ppermute | solution.py:70
  169.1 14.5 %collective-permute-start.13 = (bf16[256,512]{1,0:T(8,128)(2,1)S(1)}, bf16[256,512]{1,0:T(8,128)(2,1)S(1)}, u32[]{:S(2)}, u32[]{:S(2)}) collective-permute-start(bf16[256,512]{1,0:T(8,128)(2,1)S(1)} %collective-permute-done.11), channel_id=1, source_target_pairs={{0,2},{1,3},{2,0},{3,1},{4,6},{5,7},{6,4},{7,5},{8,10},{9,11},{10,... | collective-permute-start | bytes 786440 | tf_op jit(solution)/shard_map/ppermute | solution.py:70
  183.0 13.5 %collective-permute-start.8 = (bf16[256,512]{1,0:T(8,128)(2,1)S(1)}, bf16[256,512]{1,0:T(8,128)(2,1)S(1)}, u32[]{:S(2)}, u32[]{:S(2)}) collective-permute-start(bf16[256,512]{1,0:T(8,128)(2,1)S(1)} %add_convert_fusion.1), channel_id=1, source_target_pairs={{0,1},{1,0},{2,3},{3,2},{4,5},{5,4},{6,7},{7,6},{8,9},{9,8},{10,11... | collective-permute-start | bytes 786440 | tf_op jit(solution)/shard_map/ppermute | solution.py:70
  183.0 13.6 %collective-permute-start.12 = (bf16[256,512]{1,0:T(8,128)(2,1)S(1)}, bf16[256,512]{1,0:T(8,128)(2,1)S(1)}, u32[]{:S(2)}, u32[]{:S(2)}) collective-permute-start(bf16[256,512]{1,0:T(8,128)(2,1)S(1)} %collective-permute-done.11), channel_id=1, source_target_pairs={{0,1},{1,0},{2,3},{3,2},{4,5},{5,4},{6,7},{7,6},{8,9},{9,8},{10,11... | collective-permute-start | bytes 786440 | tf_op jit(solution)/shard_map/ppermute | solution.py:70
  183.6 13.0 %collective-permute-start.10 = (bf16[256,512]{1,0:T(8,128)(2,1)S(1)}, bf16[256,512]{1,0:T(8,128)(2,1)S(1)}, u32[]{:S(2)}, u32[]{:S(2)}) collective-permute-start(bf16[256,512]{1,0:T(8,128)(2,1)S(1)} %collective-permute-done.9), channel_id=1, source_target_pairs={{0,1},{1,0},{2,3},{3,2},{4,5},{5,4},{6,7},{7,6},{8,9},{9,8},{10,11... | collective-permute-start | bytes 786440 | tf_op jit(solution)/shard_map/ppermute | solution.py:70
  183.6 13.0 %collective-permute-start.14 = (bf16[256,512]{1,0:T(8,128)(2,1)S(1)}, bf16[256,512]{1,0:T(8,128)(2,1)S(1)}, u32[]{:S(2)}, u32[]{:S(2)}) collective-permute-start(bf16[256,512]{1,0:T(8,128)(2,1)S(1)} %collective-permute-done.13), channel_id=1, source_target_pairs={{0,1},{1,0},{2,3},{3,2},{4,5},{5,4},{6,7},{7,6},{8,9},{9,8},{10,11... | collective-permute-start | bytes 786440 | tf_op jit(solution)/shard_map/ppermute | solution.py:70
  204.0 2.0 collective-permute-start.30
  205.0 7.1 %collective-permute-start.29 = (bf16[256,1024]{1,0:T(8,128)(2,1)S(1)}, bf16[256,1024]{1,0:T(8,128)(2,1)S(1)}, u32[]{:S(2)}, u32[]{:S(2)}) collective-permute-start(bf16[256,1024]{1,0:T(8,128)(2,1)S(1)} %pad_maximum_fusion.3), channel_id=1, source_target_pairs={{0,1},{1,0},{2,3},{3,2},{4,5},{5,4},{6,7},{7,6},{8,9},{9,8},{10,11... | collective-permute-start | bytes 1572872 | tf_op jit(solution)/shard_map/ppermute | solution.py:70
  206.9 32.6 %copy-start.18 = (f32[512]{0:T(512)S(1)}, f32[512]{0:T(512)}, u32[]{:S(2)}) copy-start(f32[512]{0:T(512)} %param.41) | copy-start | bytes 6148
  206.9 32.6 %copy-start.19 = (f32[512]{0:T(512)S(1)}, f32[512]{0:T(512)}, u32[]{:S(2)}) copy-start(f32[512]{0:T(512)} %param.40) | copy-start | bytes 6148
  206.9 17.4 %collective-permute-start.31 = (bf16[256,1024]{1,0:T(8,128)(2,1)S(1)}, bf16[256,1024]{1,0:T(8,128)(2,1)S(1)}, u32[]{:S(2)}, u32[]{:S(2)}) collective-permute-start(bf16[256,1024]{1,0:T(8,128)(2,1)S(1)} %pad_maximum_fusion.5), channel_id=1, source_target_pairs={{0,8},{4,12},{8,0},{12,4},{16,24},{20,28},{24,16},{28,20},{1,9},{5... | collective-permute-start | bytes 1572872 | tf_op jit(solution)/shard_map/ppermute | solution.py:70
  224.7 7.8 %collective-permute-start.32 = (bf16[256,512]{1,0:T(8,128)(2,1)S(1)}, bf16[256,512]{1,0:T(8,128)(2,1)S(1)}, u32[]{:S(2)}, u32[]{:S(2)}) collective-permute-start(bf16[256,512]{1,0:T(8,128)(2,1)S(1)} %fusion.33), channel_id=1, source_target_pairs={{0,2},{1,3},{2,0},{3,1},{4,6},{5,7},{6,4},{7,5},{8,10},{9,11},{10,... | collective-permute-start | bytes 786440 | tf_op jit(solution)/shard_map/ppermute | solution.py:70
  (8 other events, 24.7 us)
